TPU v7x, 256 devices: a 4x2x16 block of a 4x16x16 slice. The times are simulated.
256 devices in a mesh: grp: 2 (over y), ep: 64 (over z, x), tp: 2 (over core).
Axes of the slice: x: 4, y: 2, z: 16, core: 2. Of those that a mesh axis runs over, the one named last changes fastest.
The devices are a block of a 4x16x16 slice.
Arguments:
- fresh_inputs: bfloat16 [2048, 2048], P(('grp', 'ep')), parts along dimension 0, may hold values from -6 to 6
- memory_arrays: float32 [2048, 32, 64, 64], P(('grp', 'ep'), 'tp'), parts along dimension 0, may hold values from -4 to 4
- chosen_specialist: int32 [2048, 2], P(('grp', 'ep')), parts along dimension 0, may hold values from 0 to 3, all different within a row; in each aligned block of 1024 rows (0 to 1023, 1024 to 2047, ...) at most 768 rows name the same one
- chosen_coefficient: bfloat16 [2048, 2], P(('grp', 'ep')), parts along dimension 0, may hold values from 0.25 to 1
- first_rescale: float32 [2048], replicated, may hold values from 0.1 to 1.9
- second_rescale: float32 [2048], replicated, may hold values from 0.1 to 1.9
- receiver_projector: bfloat16 [2048, 2048], P('tp', 'ep'), may hold values from -0.125 to 0.125
- address_projector: bfloat16 [2048, 2048], P('tp', 'ep'), may hold values from -0.125 to 0.125
- content_projector: bfloat16 [2048, 2048], P('tp', 'ep'), may hold values from -0.125 to 0.125
- final_projector: bfloat16 [2048, 2048], P('tp', 'ep'), may hold values from -0.125 to 0.125
- forget_narrowing: bfloat16 [2048, 64], replicated, may hold values from -0.125 to 0.125
- forget_widening: bfloat16 [64, 2048], P(None, 'tp'), may hold values from -0.75 to 0.75
- forget_bias: float32 [2048], P('tp'), may hold values from -3 to 1
- learning_narrowing: bfloat16 [2048, 64], replicated, may hold values from -0.125 to 0.125
- learning_widening: bfloat16 [64, 2048], P(None, 'tp'), may hold values from -0.75 to 0.75
- learning_bias: float32 [2048], P('tp'), may hold values from -1.5 to 1.5
- lane_scaling: float32 [2048], P('tp'), may hold values from 0.1 to 1.9
- instant_reward: float32 [32, 64], P('tp'), may hold values from -0.5 to 0.5
- specialist_switch: bfloat16 [2048, 28672], P(None, ('ep', 'tp')), may hold values from -0.125 to 0.125
- specialist_expand: bfloat16 [2048, 28672], P(None, ('ep', 'tp')), may hold values from -0.125 to 0.125
- specialist_contract: bfloat16 [28672, 2048], P(('ep', 'tp')), may hold values from -0.0625 to 0.0625
- common_activator: bfloat16 [2048, 5632], P(None, ('ep', 'tp')), may hold values from -0.125 to 0.125
- common_expand: bfloat16 [2048, 5632], P(None, ('ep', 'tp')), may hold values from -0.125 to 0.125
- common_contract: bfloat16 [5632, 2048], P(('ep', 'tp')), may hold values from -0.078125 to 0.078125
- common_switch: bfloat16 [2048], replicated, may hold values from -0.125 to 0.125
Outputs:
- new_tokens: bfloat16 [2048, 2048], P(('grp', 'ep', 'tp')), parts along dimension 0
- memory_after: float32 [2048, 32, 64, 64], P(('grp', 'ep'), 'tp'), parts along dimension 0
There are 2 independent parts, one for each index of `grp`. A program takes and returns all parts, laid end to end along the dimension named above; an argument that names none is the same for every part. Nothing has to cross between parts.
Inputs may be any that keep to these rules, and one draw needn't show every extreme that they name: `chosen_specialist`: each row names 2 different experts. Over the whole batch no expert is named by more than 768 rows, and in every draw some expert is named by exactly 768 rows.
All inputs are finite; a program needn't handle non-finite values.
Results may differ from a plain program's by a relative error of at most 0.014.
Values may be sent and summed in bfloat16 or wider, within the bound.
No kernel may reach another device: no remote copies, remote signals or barrier semaphores. Data moves between devices by JAX's collectives and lax.ppermute only.
A program may use at most 128 MiB of HBM per device.

v0:
```python
import jax
import jax.numpy as jnp
from jax import lax
from jax.sharding import Mesh
from jax.sharding import PartitionSpec as P

LANE_WIDTH = 64
FF_E = 7168
EP = ("ep_0", "ep_1")
GRP_EP = ("grp", "ep_0", "ep_1")
EP_TP = ("ep_0", "ep_1", "tp")
GRP_EP_TP = ("grp", "ep_0", "ep_1", "tp")


RMS_EPS = 1e-06
GROUP_EPS = 0.00064
HIGHEST = lax.Precision.HIGHEST


def turned_gather(arrays, axis, dims):
    turned = [jnp.moveaxis(a, dim, 0) for a, dim in zip(arrays, dims)]
    widths = [t[0].size for t in turned]
    both = jnp.concatenate([t.reshape(-1, w) for t, w in zip(turned, widths)], axis=1)
    whole = lax.all_gather(both, axis, axis=0, tiled=True)
    blocks = jnp.split(whole, [sum(widths[:k]) for k in range(1, len(widths))], axis=1)
    return tuple(
        (
            jnp.moveaxis(b.reshape(-1, *t.shape[1:]), 0, dim)
            for b, t, dim in zip(blocks, turned, dims)
        )
    )


def from_everyone(value, axis):
    copies = jnp.broadcast_to(value, (lax.axis_size(axis), *value.shape))
    return lax.all_to_all(copies, axis, split_axis=0, concat_axis=0, tiled=True)


def of_everyone(value, axis):
    return from_everyone(value, axis).astype(jnp.float32).sum(axis=0)


def whole_of(value, axes, dim):
    if not axes:
        return value
    nearer = lax.all_gather(value, axes[-1], axis=dim, tiled=True)
    return whole_of(nearer, axes[:-1], dim)


def side_by_side(arrays, axis, dim, along):
    ends, at = ([], 0)
    for a in arrays[:-1]:
        at += a.shape[along]
        ends.append(at)
    both = jnp.concatenate(arrays, axis=along)
    return tuple(jnp.split(lax.all_gather(both, axis, axis=dim, tiled=True), ends, axis=along))


def in_order(blocks, dim):
    dims = list(blocks.shape[1:])
    dims[dim] *= blocks.shape[0]
    return jnp.moveaxis(blocks, 0, dim).reshape(dims)


def one_gather(arrays, axis, dims):
    ravelled = jnp.concatenate([a.reshape(-1) for a in arrays])
    lines, at, finished = (lax.all_gather(ravelled, axis), 0, [])
    for a, dim in zip(arrays, dims):
        blocks = lines[:, at : at + a.size].reshape(-1, *a.shape)
        finished.append(in_order(blocks, dim))
        at += a.size
    return tuple(finished)


def cut_along(value, dim, devices):
    dims = value.shape
    blocks = value.reshape(*dims[:dim], devices, dims[dim] // devices, *dims[dim + 1 :])
    return jnp.moveaxis(blocks, dim, 0)


def sent_and_summed(value, axis, dim):
    devices = lax.axis_size(axis)
    blocks = lax.all_to_all(cut_along(value, dim, devices), axis, 0, 0, tiled=True)
    return jnp.sum(blocks.astype(jnp.float32), axis=0)


def rms_norm(values, norm_gain):
    mean_sq = jnp.mean(values * values, axis=-1, keepdims=True)
    return values * lax.rsqrt(mean_sq + RMS_EPS) * norm_gain


def widen(rounded):
    return lax.optimization_barrier(rounded).astype(jnp.float32)


def evolve_memory(
    memory_arrays,
    receiver_lanes,
    address_lanes,
    content_lanes,
    forget_lanes,
    learning_lanes,
    lane_rescale,
    instant_reward,
):
    unit_key = address_lanes * lax.rsqrt(
        jnp.sum(address_lanes * address_lanes, axis=-1, keepdims=True) + 1.0
    )
    stepped_address = address_lanes * learning_lanes
    removal = jnp.einsum("bhvk,bhk->bhv", memory_arrays, unit_key, precision=HIGHEST)
    memory_after = (
        memory_arrays * forget_lanes[:, :, None, :]
        - removal[..., None] * (unit_key * learning_lanes)[:, :, None, :]
        + content_lanes[..., None] * stepped_address[:, :, None, :]
    )
    memory_retrieval = jnp.einsum("bhvk,bhk->bhv", memory_after, receiver_lanes, precision=HIGHEST)
    centred = memory_retrieval - jnp.mean(memory_retrieval, axis=-1, keepdims=True)
    unit_address = centred * lax.rsqrt(
        jnp.mean(centred * centred, axis=-1, keepdims=True) + GROUP_EPS
    )
    instant_extra = (
        jnp.sum(receiver_lanes * stepped_address * instant_reward, axis=-1, keepdims=True)
        * content_lanes
    )
    return (memory_after, unit_address * lane_rescale + instant_extra)


def swiglu(rows_in, gate_w, up_w):
    gate_val = jnp.dot(rows_in, gate_w, preferred_element_type=jnp.float32)
    up_val = jnp.dot(rows_in, up_w, preferred_element_type=jnp.float32)
    return (jax.nn.silu(gate_val) * up_val).astype(jnp.bfloat16)


def body(
    fresh_inputs,
    memory_arrays,
    chosen_specialist,
    chosen_coefficient,
    first_rescale,
    second_rescale,
    receiver_projector,
    address_projector,
    content_projector,
    final_projector,
    forget_narrowing,
    forget_widening,
    forget_bias,
    learning_narrowing,
    learning_widening,
    learning_bias,
    lane_scaling,
    instant_reward,
    specialist_switch,
    specialist_expand,
    specialist_contract,
    common_activator,
    common_expand,
    common_contract,
    common_switch,
):
    own_rows = fresh_inputs.shape[0]
    model_width = fresh_inputs.shape[1]
    tp_count = lax.axis_size("tp")
    tp_rank = lax.axis_index("tp")
    half_width = model_width // tp_count
    head_count = half_width // LANE_WIDTH
    residual = fresh_inputs.astype(jnp.float32)
    normed = rms_norm(residual, first_rescale).astype(jnp.bfloat16)
    normed_half = lax.dynamic_slice_in_dim(normed, tp_rank * half_width, half_width, 1)
    pieces = turned_gather(
        (receiver_projector, address_projector, content_projector), EP, (1, 1, 1)
    )
    partials = tuple(
        (
            jnp.dot(normed_half, weight_block, preferred_element_type=jnp.float32)
            for weight_block in pieces
        )
    )
    partial_value = jnp.stack(partials, axis=1).astype(jnp.bfloat16)
    projected = (
        of_everyone(widen(partial_value).astype(jnp.bfloat16), "tp")
        .astype(jnp.float32)
        .astype(jnp.bfloat16)
    )
    mine = lax.dynamic_slice_in_dim(projected, tp_rank * half_width, half_width, 2)

    def divide_lanes(channels):
        return channels.astype(jnp.float32).reshape(own_rows, head_count, LANE_WIDTH)

    decay_mid = jnp.tanh(
        jnp.dot(normed, forget_narrowing, preferred_element_type=jnp.float32)
    ).astype(jnp.bfloat16)
    decay_pre = forget_bias + jnp.dot(
        decay_mid, forget_widening, preferred_element_type=jnp.float32
    )
    decay_vals = jnp.exp(-jnp.exp(-jax.nn.softplus(-decay_pre) - 0.5))
    rate_mid = jnp.dot(normed, learning_narrowing, preferred_element_type=jnp.float32).astype(
        jnp.bfloat16
    )
    rate_vals = jax.nn.sigmoid(
        learning_bias + jnp.dot(rate_mid, learning_widening, preferred_element_type=jnp.float32)
    )
    memory_after, memory_retrieval = evolve_memory(
        memory_arrays,
        divide_lanes(mine[:, 0]),
        divide_lanes(mine[:, 1]),
        divide_lanes(mine[:, 2]),
        divide_lanes(decay_vals),
        divide_lanes(rate_vals),
        lane_scaling.reshape(head_count, LANE_WIDTH),
        instant_reward,
    )
    attended = memory_retrieval.reshape(own_rows, half_width).astype(jnp.bfloat16)
    out_part = jnp.dot(
        attended, whole_of(final_projector, EP, 1), preferred_element_type=jnp.float32
    ).astype(jnp.bfloat16)
    mixed_out = (
        of_everyone(widen(out_part).astype(jnp.bfloat16), "tp")
        .astype(jnp.float32)
        .astype(jnp.bfloat16)
    )
    residual = residual + mixed_out.astype(jnp.float32)
    ffn_in = rms_norm(residual, second_rescale).astype(jnp.bfloat16)
    all_in, all_weight, all_ids = (
        *side_by_side((ffn_in, chosen_coefficient), EP, 0, 1),
        lax.all_gather(chosen_specialist, EP, axis=0, tiled=True),
    )
    column_count = specialist_switch.shape[1]
    flat_rank = lax.axis_index(EP) * tp_count + tp_rank
    expert = flat_rank * column_count // FF_E
    expert_share = jnp.sum(
        jnp.where(all_ids == expert, all_weight.astype(jnp.float32), 0.0), axis=1
    )
    hidden = swiglu(all_in, specialist_switch, specialist_expand)
    shared_hidden = swiglu(all_in, common_activator, common_expand)
    branch_scale = jax.nn.sigmoid(
        jnp.dot(all_in, common_switch, preferred_element_type=jnp.float32)
    )
    rows_mine = own_rows // tp_count
    hidden_pair, shared_pair = one_gather((hidden, shared_hidden), "tp", (1, 1))
    down_half, shared_half = (
        lax.all_to_all(specialist_contract, "tp", split_axis=1, concat_axis=0, tiled=True),
        lax.all_to_all(common_contract, "tp", split_axis=1, concat_axis=0, tiled=True),
    )
    half_total = expert_share[:, None] * jnp.dot(
        hidden_pair, down_half, preferred_element_type=jnp.float32
    )
    half_total = half_total + branch_scale[:, None] * jnp.dot(
        shared_pair, shared_half, preferred_element_type=jnp.float32
    )
    half_rows = sent_and_summed(half_total.astype(jnp.bfloat16), EP, 0)
    routed = lax.all_to_all(half_rows, "tp", split_axis=0, concat_axis=1, tiled=True)
    own_residual = lax.dynamic_slice_in_dim(residual, tp_rank * rows_mine, rows_mine, 0)
    return ((own_residual + routed).astype(jnp.bfloat16), memory_after)


def solution(mesh):
    torus = Mesh(
        mesh.devices.reshape(mesh.shape["grp"], 16, 4, mesh.shape["tp"]),
        ("grp", "ep_0", "ep_1", "tp"),
    )
    return jax.shard_map(
        body,
        mesh=torus,
        in_specs=(
            P(GRP_EP, None),
            P(GRP_EP, "tp", None, None),
            P(GRP_EP, None),
            P(GRP_EP, None),
            P(),
            P(),
            P("tp", EP),
            P("tp", EP),
            P("tp", EP),
            P("tp", EP),
            P(),
            P(None, "tp"),
            P("tp"),
            P(),
            P(None, "tp"),
            P("tp"),
            P("tp"),
            P("tp", None),
            P(None, EP_TP),
            P(None, EP_TP),
            P(EP_TP, None),
            P(None, EP_TP),
            P(None, EP_TP),
            P(EP_TP, None),
            P(),
        ),
        out_specs=(P(GRP_EP_TP, None), P(GRP_EP, "tp", None, None)),
        check_vma=False,
    )
```

profile of v0, /device:TPU:33, one launch (start us, length us, event | category | flops | bytes accessed | tf_op | source)
XLA Modules:
  0.0 657.6 jit_solution(10418199914732399732)
XLA Ops:
  7.3 1.7 pad_maximum_fusion.1
  9.1 12.9 %all_gather.22 = bf16[1024,128]{0,1:T(8,128)(2,1)} all-gather(bf16[1024,32]{0,1:T(8,128)(2,1)} %param.34), channel_id=1, replica_groups=mesh['grp'=2,'ep_0'=16,'ep_1'=4,'tp'=2] {'ep_1'}, dimensions={1}, use_global_device_ids=true | all-gather | bytes 327680 | tf_op jit(solution)/shard_map/all_gather | solution.py:46
  22.1 0.7 copy.70
  22.8 0.8 mul.228
  23.6 1.0 fusion.63
  24.5 0.9 fusion.65
  25.5 1.4 fusion.55
  26.9 1.4 fusion.71
  28.5 161.8 %all-gather.7.cloned.1.call-done = bf16[2048,3072]{1,0:T(8,128)(2,1)} async-done(((bf16[32,3072]{1,0:T(8,128)(2,1)}), bf16[2048,3072]{1,0:T(8,128)(2,1)}) %all-gather.7.cloned.1.call-update) | async-done | bytes 12582928 | tf_op jit(solution)/shard_map/all_gather | solution.py:24
  190.3 3.4 fusion.18
  193.6 3.5 fusion.21
  197.1 3.4 fusion.24
  200.6 6.9 %all_to_all.66 = bf16[2,16,3,2048]{3,1,2,0:T(8,128)(2,1)S(1)} all-to-all(bf16[2,16,3,2048]{3,1,2,0:T(8,128)(2,1)S(1)} %broadcast_in_dim.7), channel_id=1, replica_groups=mesh['grp'=2,'ep_0'=16,'ep_1'=4,'tp'=2] {'tp'}, dimensions={0} | all-to-all | bytes 786432 | tf_op jit(solution)/shard_map/all_to_all | solution.py:36
  207.4 0.1 reduce_sum.97
  207.5 0.1 reshape.126
  207.7 0.1 reshape.148
  208.0 0.1 multiply_reduce_fusion.2
  208.1 0.1 fusion.79
  208.2 15.4 %fusion.80 = f32[16,16,1,64]{3,2,1,0:T(1,128)S(1)} fusion(f32[16,16,64,1]{2,3,1,0:T(1,128)S(1)} %bitcast.83, f32[16,16,64,64]{3,2,1,0:T(8,128)} %param.26), kind=kOutput, calls=%fused_computation.96 | convolution fusion | flops 12582912 | bytes 4325376 | tf_op jit(solution)/shard_map/bhvk,bhk->bhv/dot_general | solution.py:110
  223.6 8.8 %multiply_add_fusion = f32[16,16,64,64]{3,2,1,0:T(8,128)S(1)} fusion(f32[16,16,64,64]{3,2,1,0:T(8,128)} %param.26, f32[16,16,64]{2,1,0:T(8,128)S(1)} %get-tuple-element.8, f32[16,16,64]{2,1,0:T(8,128)S(1)} %reshape.133, f32[16,16,64]{2,1,0:T(8,128)S(1)} %get-tuple-element.6, f32[16,16,64]{2,1,0:T(8,128)S(1)} %bitcast.82, f32[16,16,64]{2,1,0:T(8,128)S(1)} %mul.210), kind=kLoop, calls=%fused_computation.1 | loop fusion | flops 5242880 | bytes 8716288 | tf_op jit(solution)/shard_map/add | solution.py:112
  232.4 6.6 %fusion.81 = f32[16,16,1,64]{3,2,1,0:T(1,128)S(1)} fusion(f32[16,16,64,64]{3,2,1,0:T(8,128)S(1)} %multiply_add_fusion, bf16[16,16,64,1]{2,3,1,0:T(2,128)(2,1)S(1)} %reshape.148), kind=kOutput, calls=%fused_computation.97 | convolution fusion | flops 12582912 | bytes 4292608 | tf_op jit(solution)/shard_map/bhvk,bhk->bhv/dot_general | solution.py:116
  239.1 0.1 reduce_sum.99
  239.2 0.2 multiply_reduce_fusion.1
  239.4 0.5 fusion.51
  239.9 0.1 convert_element_type.105
  240.0 16.9 %all-gather.9.cloned.1.call-done = bf16[1024,2048]{0,1:T(8,128)(2,1)} async-done(((bf16[1024,128]{0,1:T(8,128)(2,1)}), bf16[1024,2048]{0,1:T(8,128)(2,1)}) %all-gather.9.cloned.1.call-update) | async-done | bytes 4194320 | tf_op jit(solution)/shard_map/all_gather | solution.py:46
  257.0 3.4 convolution_convert_fusion
  260.4 13.1 %all_to_all.67 = bf16[2,16,2048]{2,1,0:T(8,128)(2,1)S(1)} all-to-all(bf16[2,16,2048]{2,1,0:T(8,128)(2,1)S(1)} %broadcast_in_dim.8), channel_id=1, replica_groups=mesh['grp'=2,'ep_0'=16,'ep_1'=4,'tp'=2] {'tp'}, dimensions={0} | all-to-all | bytes 262144 | tf_op jit(solution)/shard_map/all_to_all | solution.py:36
  273.5 0.1 convert_add_fusion
  273.8 0.6 pad_maximum_fusion.3
  274.5 0.3 all-gather.13.cloned.1.call-start
  274.8 129.9 %all-gather.11.cloned.1.call-done = bf16[1024,2050]{1,0:T(8,128)(2,1)} async-done(((bf16[16,2050]{1,0:T(8,128)(2,1)}), bf16[1024,2050]{1,0:T(8,128)(2,1)}) %all-gather.11.cloned.1.call-update) | async-done | bytes 4198416 | tf_op jit(solution)/shard_map/all_gather | solution.py:56
  404.7 3.7 fusion.31
  408.5 1.3 fusion.46
  409.8 0.2 copy.73
  410.0 0.5 reshape.128
  410.5 3.7 fusion.35
  414.3 1.4 fusion.40
  415.8 0.2 copy.72
  416.1 1.0 reshape.127
  417.0 0.9 pad_maximum_fusion
  418.0 1.0 copy.85
  419.0 13.5 %all-to-all-start.2 = ((bf16[224,2,1024]{2,0,1:T(8,128)(2,1)}), bf16[224,2,1024]{2,0,1:T(8,128)(2,1)S(1)}, u32[]{:S(2)}, u32[]{:S(2)}) async-start(bf16[224,2,1024]{2,0,1:T(8,128)(2,1)} %bitcast.75), calls=%async_computation.2 | async-start | bytes 1835008 | tf_op jit(solution)/shard_map/all_to_all | solution.py:242
  432.5 61.6 %all-gather.1 = s32[64,16,2]{1,2,0:T(2,128)S(1)} all-gather(s32[1,16,2]{1,2,0:T(2,128)S(1)} %bitcast.90), channel_id=1, replica_groups=mesh['grp'=2,'ep_0'=16,'ep_1'=4,'tp'=2] {'ep_0','ep_1'}, dimensions={0}, use_global_device_ids=true | all-gather | bytes 8320 | tf_op jit(solution)/shard_map/all_gather | solution.py:226
  494.2 0.1 copy.69
  494.3 0.1 reshape.138
  494.5 0.7 copy.77
  495.3 0.1 copy.82
  495.4 3.4 fusion.27
  498.8 1.5 reshape.134
  500.4 0.1 slice.21
  500.5 0.7 slice.20
  501.2 1.4 reshape.129
  502.6 1.3 copy.74
  503.9 1.5 reshape.130
  505.4 0.2 copy.76
  505.7 22.6 %all-to-all-start.3 = ((bf16[44,2,1024]{2,0,1:T(8,128)(2,1)}), bf16[44,2,1024]{2,0,1:T(8,128)(2,1)S(1)}, u32[]{:S(2)}, u32[]{:S(2)}) async-start(bf16[44,2,1024]{2,0,1:T(8,128)(2,1)} %copy.77), calls=%async_computation.3 | async-start | bytes 393216 | tf_op jit(solution)/shard_map/all_to_all | solution.py:243
  528.2 4.4 fusion.58
  532.7 4.4 fusion.8
  537.0 9.9 %all-to-all-start.4 = ((bf16[64,16,1024]{2,1,0:T(8,128)(2,1)}), bf16[64,16,1024]{2,1,0:T(8,128)(2,1)S(1)}, u32[]{:S(2)}, u32[]{:S(2)}) async-start(bf16[64,16,1024]{2,1,0:T(8,128)(2,1)} %bitcast.20), calls=%async_computation.4 | async-start | bytes 4194304 | tf_op jit(solution)/shard_map/all_to_all | solution.py:83
  546.9 95.3 %all-to-all-done.4 = bf16[64,16,1024]{2,1,0:T(8,128)(2,1)S(1)} async-done(((bf16[64,16,1024]{2,1,0:T(8,128)(2,1)}), bf16[64,16,1024]{2,1,0:T(8,128)(2,1)S(1)}, u32[]{:S(2)}, u32[]{:S(2)}) %all-to-all-start.4) | async-done | bytes 2097184 | tf_op jit(solution)/shard_map/all_to_all | solution.py:83
  642.3 0.4 convert_reduce_fusion
  642.6 7.9 %all_to_all.68 = f32[2,8,1024]{2,1,0:T(8,128)S(1)} all-to-all(f32[2,8,1024]{2,1,0:T(8,128)S(1)} %bitcast.84), channel_id=1, replica_groups=mesh['grp'=2,'ep_0'=16,'ep_1'=4,'tp'=2] {'tp'}, dimensions={0} | all-to-all | bytes 131072 | tf_op jit(solution)/shard_map/all_to_all | solution.py:252
  650.5 0.6 add_convert_fusion
  (66 shorter events, 1.3 us)
Async XLA Ops:
  7.2 403.3 %copy-start = (bf16[2048,224]{0,1:T(8,128)(2,1)S(1)}, bf16[2048,224]{0,1:T(8,128)(2,1)}, u32[]{:S(2)}) copy-start(bf16[2048,224]{0,1:T(8,128)(2,1)} %param.43) | copy-start | bytes 2752516
  7.2 183.1 %all-gather.7.cloned.1.call-start = ((), (), s32[]{:S(2)}) async-start(), calls=%async_computation.6 | async-start | bytes 12779520 | tf_op jit(solution)/shard_map/all_gather | solution.py:24
  9.0 248.0 %all-gather.9.cloned.1.call-start = ((), (), s32[]{:S(2)}) async-start(), calls=%async_computation.7 | async-start | bytes 4456448 | tf_op jit(solution)/shard_map/all_gather | solution.py:46
  22.0 382.7 %all-gather.11.cloned.1.call-start = ((), (), s32[]{:S(2)}) async-start(), calls=%async_computation.8 | async-start | bytes 4526080 | tf_op jit(solution)/shard_map/all_gather | solution.py:56
  232.4 6.6 %copy-start.2 = (f32[16,16,64,64]{3,2,1,0:T(8,128)}, f32[16,16,64,64]{3,2,1,0:T(8,128)S(1)}, u32[]{:S(2)}) copy-start(f32[16,16,64,64]{3,2,1,0:T(8,128)S(1)} %multiply_add_fusion) | copy-start | bytes 12582916
  232.4 7.0 %copy-start.7 = (f32[16,64]{1,0:T(8,128)S(1)}, f32[16,64]{1,0:T(8,128)}, u32[]{:S(2)}) copy-start(f32[16,64]{1,0:T(8,128)} %param.42) | copy-start | bytes 12292
  239.0 34.5 %copy-start.4 = (bf16[16,2048]{1,0:T(8,128)(2,1)S(1)}, bf16[16,2048]{1,0:T(8,128)(2,1)}, u32[]{:S(2)}) copy-start(bf16[16,2048]{1,0:T(8,128)(2,1)} %param.25) | copy-start | bytes 196612
  239.0 34.7 %copy-start.8 = (f32[2048]{0:T(1024)S(1)}, f32[2048]{0:T(1024)}, u32[]{:S(2)}) copy-start(f32[2048]{0:T(1024)} %param.30) | copy-start | bytes 24580
  239.0 165.7 %copy-start.12 = (bf16[2048,44]{0,1:T(8,128)(2,1)S(1)}, bf16[2048,44]{0,1:T(8,128)(2,1)}, u32[]{:S(2)}) copy-start(bf16[2048,44]{0,1:T(8,128)(2,1)} %param.46) | copy-start | bytes 540676
  274.5 134.0 %copy-start.13 = (bf16[2048,44]{0,1:T(8,128)(2,1)S(1)}, bf16[2048,44]{0,1:T(8,128)(2,1)}, u32[]{:S(2)}) copy-start(bf16[2048,44]{0,1:T(8,128)(2,1)} %param.47) | copy-start | bytes 540676
  274.5 224.3 %all-gather.13.cloned.1.call-start = ((), (), s32[]{:S(2)}) async-start(), calls=%async_computation.9 | async-start | bytes 1646592 | tf_op jit(solution)/shard_map/all_gather | solution.py:67
  404.7 3.7 copy-start.3
  410.0 4.3 slice-start
  410.5 3.8 slice-start.1
  410.5 3.8 copy-start.11
  415.8 2.2 copy-start.5
  415.8 16.7 %copy-start.9 = (bf16[2048]{0:T(1024)(128)(2,1)S(1)}, bf16[2048]{0:T(1024)(128)(2,1)}, u32[]{:S(2)}) copy-start(bf16[2048]{0:T(1024)(128)(2,1)} %param.49) | copy-start | bytes 12292
  415.8 16.7 %copy-start.10 = (s32[16,2]{0,1:T(2,128)S(1)}, s32[16,2]{0,1:T(2,128)}, u32[]{:S(2)}) copy-start(s32[16,2]{0,1:T(2,128)} %param.27) | copy-start | bytes 388
  415.8 78.6 %copy-start.6 = (bf16[44,2048]{1,0:T(8,128)(2,1)S(1)}, bf16[44,2048]{1,0:T(8,128)(2,1)}, u32[]{:S(2)}) copy-start(bf16[44,2048]{1,0:T(8,128)(2,1)} %param.48) | copy-start | bytes 540676
  415.8 79.4 %slice-start.2 = ((bf16[1024,2050]{1,0:T(8,128)(2,1)}), bf16[1024,2]{1,0:T(8,128)(2,1)S(1)}, s32[]{:S(2)}) async-start(bf16[1024,2050]{1,0:T(8,128)(2,1)} %all-gather.11.cloned.1.call-done), calls=%async_computation.12 | async-start | bytes 524288 | tf_op jit(solution)/shard_map/split | solution.py:56
  419.0 86.7 %all-to-all-start.2 = ((bf16[224,2,1024]{2,0,1:T(8,128)(2,1)}), bf16[224,2,1024]{2,0,1:T(8,128)(2,1)S(1)}, u32[]{:S(2)}, u32[]{:S(2)}) async-start(bf16[224,2,1024]{2,0,1:T(8,128)(2,1)} %bitcast.75), calls=%async_computation.2 | async-start | bytes 1835008 | tf_op jit(solution)/shard_map/all_to_all | solution.py:242
  505.7 27.0 %all-to-all-start.3 = ((bf16[44,2,1024]{2,0,1:T(8,128)(2,1)}), bf16[44,2,1024]{2,0,1:T(8,128)(2,1)S(1)}, u32[]{:S(2)}, u32[]{:S(2)}) async-start(bf16[44,2,1024]{2,0,1:T(8,128)(2,1)} %copy.77), calls=%async_computation.3 | async-start | bytes 393216 | tf_op jit(solution)/shard_map/all_to_all | solution.py:243
  532.7 118.5 %copy-start.1 = (bf16[2048,224]{0,1:T(8,128)(2,1)S(1)}, bf16[2048,224]{0,1:T(8,128)(2,1)}, u32[]{:S(2)}) copy-start(bf16[2048,224]{0,1:T(8,128)(2,1)} %param.43) | copy-start | bytes 2752516
  537.0 105.3 %all-to-all-start.4 = ((bf16[64,16,1024]{2,1,0:T(8,128)(2,1)}), bf16[64,16,1024]{2,1,0:T(8,128)(2,1)S(1)}, u32[]{:S(2)}, u32[]{:S(2)}) async-start(bf16[64,16,1024]{2,1,0:T(8,128)(2,1)} %bitcast.20), calls=%async_computation.4 | async-start | bytes 4194304 | tf_op jit(solution)/shard_map/all_to_all | solution.py:83
Sparse Core Ops, SparseCore 0:
  11.0 179.2 all-gather.6
  192.1 64.8 all-gather.8
  274.6 130.0 all-gather.10
  418.1 23.4 all-gather.12
where the time goes:
time: 659 us; the launch traced here: 658 us
  waiting for transfers between devices  404 us (61%)
  blocking collectives  102 us (15%)
  matrix products  60.8 us (9%)
  starting transfers between devices  46.5 us (7%)
  other arithmetic  16.3 us (2%)
  between operations  14.3 us (2%)
  local copies, waits for them, and re-layouts  13.2 us (2%)
    all_gather x1, waiting for transfers between devices, turned_gather(): whole = lax.all_gather(both, axis, axis=0, tiled=True)  162 us
    all_gather x1, waiting for transfers between devices, side_by_side(): lax.all_gather(both, axis, axis=dim, tiled=True)  130 us
    all_to_all x1, waiting for transfers between devices, sent_and_summed(): lax.all_to_all(cut_along(value, dim, devices), axis, 0, 0, tiled=True)  95.3 us
    all_gather x1, blocking collectives, body(): lax.all_gather(chosen_specialist, EP, axis=0, tiled=True)  61.6 us
    all_to_all x1, starting transfers between devices, body(): lax.all_to_all(common_contract, 'tp', split_axis=1, concat_axis=0, tiled=...  22.6 us
    all_to_all x2, blocking collectives, from_everyone(): return lax.all_to_all(copies, axis, split_axis=0, concat_axis=0, tiled=True)  20 us
    all_gather x1, waiting for transfers between devices, whole_of(): nearer = lax.all_gather(value, axes[-1], axis=dim, tiled=True)  16.9 us
    dot_general x1, matrix products, evolve_memory(): jnp.einsum('bhvk,bhk->bhv', memory_arrays, unit_key, precision=HIGHEST)  15.4 us
  transfers between devices with their start and end apart: 7, of which 4 were waited for; matrix products, arithmetic and copies ran while one was open for 10% of the time, Pallas kernels for 0%

commit v1 on v0

v1 whole, which is shorter than its diff:
```python
import jax
import jax.numpy as jnp
from jax import lax
from jax.sharding import Mesh
from jax.sharding import PartitionSpec as P


LANE_WIDTH = 64
FF_E = 7168
EP = ("ep_0", "ep_1")
GRP_EP = ("grp", "ep_0", "ep_1")
EP_TP = ("ep_0", "ep_1", "tp")
GRP_EP_TP = ("grp", "ep_0", "ep_1", "tp")


RMS_EPS = 1e-06
GROUP_EPS = 0.00064
HIGHEST = lax.Precision.HIGHEST
BF16 = jnp.bfloat16
F32 = jnp.float32


def from_ahead(value, axis, steps):
    size = lax.axis_size(axis)
    return lax.ppermute(value, axis, [((i + steps) % size, i) for i in range(size)])


def row_pieces(value, axis):
    return [value] + [from_ahead(value, axis, k) for k in range(1, lax.axis_size(axis))]


def in_row_order(pieces, axis):
    count = len(pieces)
    start = (count - lax.axis_index(axis)) % count
    twice = jnp.stack(pieces + pieces[:-1])
    return lax.dynamic_slice_in_dim(twice, start, count, 0)


def rms_norm(values, norm_gain):
    mean_sq = jnp.mean(values * values, axis=-1, keepdims=True)
    return values * lax.rsqrt(mean_sq + RMS_EPS) * norm_gain


def evolve_memory(
    memory_arrays,
    receiver_lanes,
    address_lanes,
    content_lanes,
    forget_lanes,
    learning_lanes,
    lane_rescale,
    instant_reward,
):
    unit_key = address_lanes * lax.rsqrt(
        jnp.sum(address_lanes * address_lanes, axis=-1, keepdims=True) + 1.0
    )
    stepped_address = address_lanes * learning_lanes
    removal = jnp.einsum("bhvk,bhk->bhv", memory_arrays, unit_key, precision=HIGHEST)
    memory_after = (
        memory_arrays * forget_lanes[:, :, None, :]
        - removal[..., None] * (unit_key * learning_lanes)[:, :, None, :]
        + content_lanes[..., None] * stepped_address[:, :, None, :]
    )
    memory_retrieval = jnp.einsum("bhvk,bhk->bhv", memory_after, receiver_lanes, precision=HIGHEST)
    centred = memory_retrieval - jnp.mean(memory_retrieval, axis=-1, keepdims=True)
    unit_address = centred * lax.rsqrt(
        jnp.mean(centred * centred, axis=-1, keepdims=True) + GROUP_EPS
    )
    instant_extra = (
        jnp.sum(receiver_lanes * stepped_address * instant_reward, axis=-1, keepdims=True)
        * content_lanes
    )
    return (memory_after, unit_address * lane_rescale + instant_extra)


def rows_dot(left, right_rows):
    return lax.dot_general(left, right_rows, (((1,), (1,)), ((), ())), preferred_element_type=F32)


def body(
    fresh_inputs,
    memory_arrays,
    chosen_specialist,
    chosen_coefficient,
    first_rescale,
    second_rescale,
    receiver_projector,
    address_projector,
    content_projector,
    final_projector,
    forget_narrowing,
    forget_widening,
    forget_bias,
    learning_narrowing,
    learning_widening,
    learning_bias,
    lane_scaling,
    instant_reward,
    specialist_switch,
    specialist_expand,
    specialist_contract,
    common_activator,
    common_expand,
    common_contract,
    common_switch,
):
    own_rows, model_width = fresh_inputs.shape
    tp_count = lax.axis_size("tp")
    tp_rank = lax.axis_index("tp")
    z_count = lax.axis_size("ep_0")
    half_width = model_width // tp_count
    head_count = half_width // LANE_WIDTH
    half_rows = own_rows // tp_count
    swap = [(0, 1), (1, 0)]

    final_row = in_row_order(row_pieces(final_projector.T, "ep_1"), "ep_1")
    qkv_rows = jnp.stack((receiver_projector.T, address_projector.T, content_projector.T))
    qkv_row = in_row_order(row_pieces(qkv_rows, "ep_1"), "ep_1")
    qkv_row = jnp.swapaxes(qkv_row, 0, 1).reshape(-1, half_width)
    final_whole = lax.all_gather(
        final_row.reshape(-1, half_width), "ep_0", axis=0, tiled=True
    )

    expert_cols = specialist_switch.shape[1]
    common_cols = common_activator.shape[1]
    pad = ((0, -common_cols % 16), (0, 0))
    block = expert_cols + common_cols + pad[0][1]
    bulk = jnp.concatenate(
        (
            specialist_switch.T,
            jnp.pad(common_activator.T, pad),
            specialist_expand.T,
            jnp.pad(common_expand.T, pad),
            specialist_contract,
            jnp.pad(common_contract, pad),
        )
    )
    bulks = row_pieces(bulk, "ep_1")

    residual = fresh_inputs.astype(F32)
    normed = rms_norm(residual, first_rescale).astype(BF16)
    normed_half = lax.dynamic_slice_in_dim(normed, tp_rank * half_width, half_width, 1)
    names = lax.broadcasted_iota(jnp.int32, (own_rows, 128), 1)
    share_table = jnp.zeros((own_rows, 128), F32)
    for k in range(chosen_specialist.shape[1]):
        share_table += jnp.where(
            chosen_specialist[:, k : k + 1] == names, chosen_coefficient[:, k : k + 1].astype(F32), 0.0
        )
    ring_own = jnp.concatenate((normed_half, share_table.astype(BF16)), axis=1)
    ring = lax.all_gather(ring_own, "ep_0", axis=0, tiled=True)
    ring_half, ring_share = ring[:, :half_width], ring[:, half_width:]

    partial = rows_dot(ring_half, qkv_row).astype(BF16)
    partial = lax.all_to_all(
        partial.reshape(z_count, own_rows, -1), "ep_0", 0, 0, tiled=True
    ).reshape(z_count, own_rows, 3, -1)
    partial = jnp.transpose(partial, (2, 1, 0, 3)).reshape(3, own_rows, model_width)
    keep = lax.dynamic_slice_in_dim(partial, tp_rank * half_width, half_width, 2)
    give = lax.dynamic_slice_in_dim(partial, (1 - tp_rank) * half_width, half_width, 2)
    got = lax.ppermute(give, "tp", swap)
    mine = (keep.astype(F32) + got.astype(F32)).astype(BF16)

    def divide_lanes(channels):
        return channels.astype(F32).reshape(own_rows, head_count, LANE_WIDTH)

    decay_mid = jnp.tanh(
        jnp.dot(normed, forget_narrowing, preferred_element_type=F32)
    ).astype(BF16)
    decay_pre = forget_bias + jnp.dot(decay_mid, forget_widening, preferred_element_type=F32)
    decay_vals = jnp.exp(-jnp.exp(-jax.nn.softplus(-decay_pre) - 0.5))
    rate_mid = jnp.dot(normed, learning_narrowing, preferred_element_type=F32).astype(BF16)
    rate_vals = jax.nn.sigmoid(
        learning_bias + jnp.dot(rate_mid, learning_widening, preferred_element_type=F32)
    )
    memory_after, memory_retrieval = evolve_memory(
        memory_arrays,
        divide_lanes(mine[0]),
        divide_lanes(mine[1]),
        divide_lanes(mine[2]),
        divide_lanes(decay_vals),
        divide_lanes(rate_vals),
        lane_scaling.reshape(head_count, LANE_WIDTH),
        instant_reward,
    )
    attended = memory_retrieval.reshape(own_rows, half_width).astype(BF16)
    out_part = rows_dot(attended, final_whole).astype(BF16)
    out_other = lax.ppermute(out_part, "tp", swap)
    mixed_out = (out_part.astype(F32) + out_other.astype(F32)).astype(BF16)
    residual = residual + mixed_out.astype(F32)
    ffn_in = rms_norm(residual, second_rescale).astype(BF16)
    own_in = lax.dynamic_slice_in_dim(ffn_in, tp_rank * half_rows, half_rows, 0)
    ring_in = lax.all_gather(own_in, "ep_0", axis=0, tiled=True)
    other_in = lax.ppermute(ring_in, "tp", swap)
    all_in = jnp.concatenate((ring_in, other_in))

    flat_rank = lax.axis_index(EP) * tp_count + tp_rank
    expert = flat_rank * expert_cols // FF_E
    ring_names = lax.broadcasted_iota(jnp.int32, ring_share.shape, 1)
    expert_share = jnp.sum(
        jnp.where(ring_names == expert, ring_share.astype(F32), 0.0), axis=1
    ).reshape(z_count, tp_count, half_rows)
    expert_share = jnp.concatenate(
        [
            lax.dynamic_slice_in_dim(expert_share, rank, 1, 1).reshape(-1)
            for rank in (tp_rank, 1 - tp_rank)
        ]
    )
    branch_scale = jax.nn.sigmoid(jnp.dot(all_in, common_switch, preferred_element_type=F32))
    columns = lax.broadcasted_iota(jnp.int32, (all_in.shape[0], block), 1)
    scale = jnp.where(columns < expert_cols, expert_share[:, None], branch_scale[:, None])
    total = None
    for piece in bulks:
        gate_val = rows_dot(all_in, piece[:block])
        up_val = rows_dot(all_in, piece[block : 2 * block])
        hidden = (jax.nn.silu(gate_val) * up_val * scale).astype(BF16)
        term = jnp.dot(hidden, piece[2 * block :], preferred_element_type=F32)
        total = term if total is None else total + term
    ring_rows = ring_in.shape[0]
    other_total = lax.ppermute(total[ring_rows:].astype(BF16), "tp", swap)
    ring_total = (total[:ring_rows] + other_total.astype(F32)).astype(BF16)
    blocks = lax.all_to_all(
        ring_total.reshape(z_count, half_rows, model_width), "ep_0", 0, 0, tiled=True
    )
    routed = jnp.sum(blocks.astype(F32), axis=0)
    own_residual = lax.dynamic_slice_in_dim(residual, tp_rank * half_rows, half_rows, 0)
    return ((own_residual + routed).astype(BF16), memory_after)


def solution(mesh):
    torus = Mesh(
        mesh.devices.reshape(mesh.shape["grp"], 16, 4, mesh.shape["tp"]),
        ("grp", "ep_0", "ep_1", "tp"),
    )
    return jax.shard_map(
        body,
        mesh=torus,
        in_specs=(
            P(GRP_EP, None),
            P(GRP_EP, "tp", None, None),
            P(GRP_EP, None),
            P(GRP_EP, None),
            P(),
            P(),
            P("tp", EP),
            P("tp", EP),
            P("tp", EP),
            P("tp", EP),
            P(),
            P(None, "tp"),
            P("tp"),
            P(),
            P(None, "tp"),
            P("tp"),
            P("tp"),
            P("tp", None),
            P(None, EP_TP),
            P(None, EP_TP),
            P(EP_TP, None),
            P(None, EP_TP),
            P(None, EP_TP),
            P(EP_TP, None),
            P(),
        ),
        out_specs=(P(GRP_EP_TP, None), P(GRP_EP, "tp", None, None)),
        check_vma=False,
    )
```

time: 659 us -> 314 us (0.48)
  waiting for transfers between devices: 404 us -> 44.2 us
  blocking collectives: 102 us -> 116 us
    all_gather x4 -> x1, waiting for transfers between devices: 309 us -> 0.02 us  [body(): lax.all_gather(final_row.reshape(-1, half_width), 'ep_0', axis=0, tiled=T...]
    all_to_all x3 -> x1, waiting for transfers between devices: 95.3 us -> 8.26 us  [body(): lax.all_to_all(partial.reshape(z_count, own_rows, -1), 'ep_0', 0, 0, tile...]
    ppermute x0 -> x13, starting transfers between devices: none -> 47.5 us  [the longest x1 22.8 us: body(): other_total = lax.ppermute(total[ring_rows:].astype(BF16), 'tp', swap)]
    all_to_all x3 -> x1, starting transfers between devices: 46 us -> 3.96 us  [body(): lax.all_to_all(partial.reshape(z_count, own_rows, -1), 'ep_0', 0, 0, tile...]
    ppermute x0 -> x13, waiting for transfers between devices: none -> 35.9 us  [the longest x9 32.1 us: from_ahead(): lax.ppermute(value, axis, [((i + steps) % size, i) for i in range(size)])]
    all_gather x2, blocking collectives: 74.5 us -> 81.9 us  [the longest x1 53.4 us: body(): ring = lax.all_gather(ring_own, 'ep_0', axis=0, tiled=True)]
    all_to_all x3 -> x1, blocking collectives: 27.8 us -> 33.6 us  [body(): lax.all_to_all(ring_total.reshape(z_count, half_rows, model_width), 'ep_0...]
  transfers between devices with their start and end apart: 7 -> 15, of which waited for: 4 -> 8; matrix products, arithmetic and copies ran while one was open for 10% -> 21% of each run, Pallas kernels for 0% -> 0%
where the time goes in v1:
time: 314 us; the launch traced here: 308 us
  blocking collectives  116 us (37%)
  matrix products  55.9 us (18%)
  starting transfers between devices  51.6 us (16%)
  waiting for transfers between devices  44.2 us (14%)
  between operations  14.8 us (5%)
  other arithmetic  13.5 us (4%)
  local copies, waits for them, and re-layouts  12.5 us (4%)
    all_gather x1, blocking collectives, body(): ring = lax.all_gather(ring_own, 'ep_0', axis=0, tiled=True)  53.4 us
    all_to_all x1, blocking collectives, body(): lax.all_to_all(ring_total.reshape(z_count, half_rows, model_width), 'ep_0...  33.6 us
    ppermute x9, waiting for transfers between devices, from_ahead(): lax.ppermute(value, axis, [((i + steps) % size, i) for i in range(size)])  32.1 us
    all_gather x1, blocking collectives, body(): ring_in = lax.all_gather(own_in, 'ep_0', axis=0, tiled=True)  28.6 us
    ppermute x1, starting transfers between devices, body(): other_total = lax.ppermute(total[ring_rows:].astype(BF16), 'tp', swap)  22.8 us
    dot_general x4, matrix products, body(): term = jnp.dot(hidden, piece[2 * block:], preferred_element_type=F32)  18.6 us
    dot_general x1, matrix products, evolve_memory(): jnp.einsum('bhvk,bhk->bhv', memory_arrays, unit_key, precision=HIGHEST)  15.4 us
    dot_general x6, matrix products, rows_dot(): lax.dot_general(left, right_rows, (((1,), (1,)), ((), ())), preferred_ele...  14.1 us
  transfers between devices with their start and end apart: 15, of which 8 were waited for; matrix products, arithmetic and copies ran while one was open for 21% of the time, Pallas kernels for 0%

profile of v1, /device:TPU:33, one launch (start us, length us, event | category | flops | bytes accessed | tf_op | source)
XLA Modules:
  0.0 308.0 jit_solution(12477992935292290480)
XLA Ops:
  7.3 1.0 pad_maximum_fusion
  8.3 3.8 %collective-permute-start = (bf16[3,32,1024]{2,1,0:T(8,128)(2,1)S(1)}, bf16[3,32,1024]{2,1,0:T(8,128)(2,1)S(1)}, u32[]{:S(2)}, u32[]{:S(2)}) collective-permute-start(bf16[3,32,1024]{2,1,0:T(8,128)(2,1)S(1)} %pad_maximum_fusion), channel_id=1, source_target_pairs={{2,0},{4,2},{6,4},{0,6},{3,1},{5,3},{7,5},{1,7},{10,8},{12,10},{14... | collective-permute-start | bytes 589832 | tf_op jit(solution)/shard_map/ppermute | solution.py:25
  12.1 0.3 collective-permute-start.1
  12.4 0.7 collective-permute-start.2
  13.1 2.0 collective-permute-start.4
  15.1 1.5 collective-permute-start.5
  16.6 0.9 bitcast_dynamic-update-slice_fusion.7
  17.4 2.3 constant_dynamic-update-slice_fusion.7
  19.7 0.1 fusion.82
  20.0 0.1 collective-permute-start.6
  20.2 0.8 collective-permute-done.5
  21.0 3.5 %collective-permute-done.6 = bf16[32,1024]{1,0:T(8,128)(2,1)S(1)} collective-permute-done((bf16[32,1024]{1,0:T(8,128)(2,1)S(1)}, bf16[32,1024]{1,0:T(8,128)(2,1)S(1)}, u32[]{:S(2)}, u32[]{:S(2)}) %collective-permute-start.6) | collective-permute-done | bytes 65568 | tf_op jit(solution)/shard_map/ppermute | solution.py:25
  24.6 0.7 constant_dynamic-slice_fusion
  25.5 0.8 fusion.101
  26.2 1.0 constant_dynamic-update-slice_fusion.5
  27.3 53.4 %all_gather.9 = bf16[256,1152]{1,0:T(8,128)(2,1)S(1)} all-gather(bf16[16,1152]{1,0:T(8,128)(2,1)S(1)} %pad_maximum_fusion.1), channel_id=1, replica_groups=mesh['grp'=2,'ep_0'=16,'ep_1'=4,'tp'=2] {'ep_0'}, dimensions={0}, use_global_device_ids=true | all-gather | bytes 626688 | tf_op jit(solution)/shard_map/all_gather | solution.py:150
  80.9 1.1 convolution_convert_fusion.1
  82.1 4.0 %all-to-all-start = ((bf16[16,16,384]{2,1,0:T(8,128)(2,1)}), bf16[16,16,384]{2,1,0:T(8,128)(2,1)S(1)}, u32[]{:S(2)}, u32[]{:S(2)}) async-start(bf16[16,16,384]{2,1,0:T(8,128)(2,1)} %bitcast.21), calls=%async_computation | async-start | bytes 393216 | tf_op jit(solution)/shard_map/all_to_all | solution.py:154
  86.1 0.8 fusion.100
  86.9 1.0 constant_dynamic-update-slice_fusion.3
  87.9 0.8 fusion.102
  88.7 2.7 collective-permute-start.9
  91.4 0.4 fusion.8
  91.7 8.3 %all-to-all-done = bf16[16,16,384]{2,1,0:T(8,128)(2,1)S(1)} async-done(((bf16[16,16,384]{2,1,0:T(8,128)(2,1)}), bf16[16,16,384]{2,1,0:T(8,128)(2,1)S(1)}, u32[]{:S(2)}, u32[]{:S(2)}) %all-to-all-start) | async-done | bytes 196640 | tf_op jit(solution)/shard_map/all_to_all | solution.py:154
  100.0 0.2 copy.32
  100.3 8.6 %collective-permute-start.3 = (bf16[3,16,1024]{2,1,0:T(8,128)(2,1)S(1)}, bf16[3,16,1024]{2,1,0:T(8,128)(2,1)S(1)}, u32[]{:S(2)}, u32[]{:S(2)}) collective-permute-start(bf16[3,16,1024]{2,1,0:T(8,128)(2,1)S(1)} %constant_dynamic-slice_fusion.1), channel_id=1, source_target_pairs={{0,1},{1,0},{2,3},{3,2},{4,5},{5,4},{6,7},{7,6},{8,9},{9,8},{10,11... | collective-permute-start | bytes 294920 | tf_op jit(solution)/shard_map/ppermute | solution.py:160
  109.0 0.4 fusion.90
  109.7 0.2 collective-permute-done.3
  110.0 0.1 reshape.148
  110.1 0.1 reshape.131
  110.4 0.1 multiply_reduce_fusion.2
  110.6 15.4 %fusion.104 = f32[16,16,1,64]{3,2,1,0:T(1,128)S(1)} fusion(f32[16,16,64,1]{2,3,1,0:T(1,128)S(1)} %bitcast.116, f32[16,16,64,64]{3,2,1,0:T(8,128)} %param.26), kind=kOutput, calls=%fused_computation.161 | convolution fusion | flops 12582912 | bytes 4325376 | tf_op jit(solution)/shard_map/bhvk,bhk->bhv/dot_general | solution.py:58
  126.1 8.7 %multiply_add_fusion = f32[16,16,64,64]{3,2,1,0:T(8,128)S(1)} fusion(f32[16,16,64,64]{3,2,1,0:T(8,128)} %param.26, f32[16,16,64]{2,1,0:T(8,128)S(1)} %get-tuple-element.8, f32[16,16,64]{2,1,0:T(8,128)S(1)} %reshape.140, f32[16,16,64]{2,1,0:T(8,128)S(1)} %get-tuple-element.6, f32[16,16,64]{2,1,0:T(8,128)S(1)} %bitcast.115, f32[16,16,64]{2,1,0:T(8,128)S(1)} %mul.221), kind=kLoop, calls=%fused_computation.1 | loop fusion | flops 5242880 | bytes 8716288 | tf_op jit(solution)/shard_map/add | solution.py:60
  134.8 6.6 %fusion.105 = f32[16,16,1,64]{3,2,1,0:T(1,128)S(1)} fusion(f32[16,16,64,64]{3,2,1,0:T(8,128)S(1)} %multiply_add_fusion, bf16[16,16,64,1]{2,3,1,0:T(2,128)(2,1)S(1)} %reshape.148), kind=kOutput, calls=%fused_computation.162 | convolution fusion | flops 12582912 | bytes 4292608 | tf_op jit(solution)/shard_map/bhvk,bhk->bhv/dot_general | solution.py:64
  141.4 0.1 reduce_sum.74
  141.5 0.2 multiply_reduce_fusion.1
  141.8 0.5 fusion.4
  142.3 0.1 convert_element_type.141
  142.4 3.4 %convolution_convert_fusion = bf16[16,2048]{1,0:T(8,128)(2,1)S(1)} fusion(bf16[16,1024]{1,0:T(8,128)(2,1)S(1)} %convert_element_type.141, bf16[2048,1024]{1,0:T(8,128)(2,1)} %all-gather.2.cloned.1.call-done), kind=kOutput, calls=%fused_computation.5 | convolution fusion | flops 67141632 | bytes 4292608 | tf_op jit(solution)/shard_map/dot_general | solution.py:77
  145.8 0.4 collective-permute-start.7
  146.2 0.9 collective-permute-done.7
  147.1 0.1 multiply_reduce_fusion
  147.4 28.6 %all_gather.11 = bf16[128,2048]{1,0:T(8,128)(2,1)S(1)} all-gather(bf16[8,2048]{1,0:T(8,128)(2,1)S(1)} %multiply_convert_fusion), channel_id=1, replica_groups=mesh['grp'=2,'ep_0'=16,'ep_1'=4,'tp'=2] {'ep_0'}, dimensions={0}, use_global_device_ids=true | all-gather | bytes 557056 | tf_op jit(solution)/shard_map/all_gather | solution.py:192
  176.0 4.7 %collective-permute-start.8 = (bf16[128,2048]{1,0:T(8,128)(2,1)S(1)}, bf16[128,2048]{1,0:T(8,128)(2,1)}, u32[]{:S(2)}, u32[]{:S(2)}) collective-permute-start(bf16[128,2048]{1,0:T(8,128)(2,1)S(1)} %all_gather.11), channel_id=1, source_target_pairs={{0,1},{1,0},{2,3},{3,2},{4,5},{5,4},{6,7},{7,6},{8,9},{9,8},{10,11... | collective-permute-start | bytes 1572872 | tf_op jit(solution)/shard_map/ppermute | solution.py:193
  180.7 0.1 select_reduce_fusion
  180.8 0.1 reshape.133
  181.2 1.1 collective-permute-done.8
  182.4 1.1 constant_dynamic-update-slice_fusion
  183.4 0.4 fusion.106
  183.8 2.1 fusion.26
  186.0 2.6 fusion.12
  188.6 2.5 fusion.22
  191.1 4.1 %fusion.34 = f32[256,2048]{1,0:T(8,128)} fusion(bf16[48,2048]{1,0:T(8,128)(2,1)} %get-tuple-element.13, bf16[224,2048]{1,0:T(8,128)(2,1)S(1)} %copy-done.6, f32[256,272]{0,1:T(8,128)} %fusion.26, bf16[256,2048]{1,0:T(8,128)(2,1)S(1)} %constant_dynamic-update-slice_fusion, bf16[48,2048]{1,0:T(8,128)(2,1)S(1)} %copy-done.16, ...), kind=kOutput, calls=%fused_computation.41 | convolution fusion | flops 575438848 | bytes 5654800 | tf_op jit(solution)/shard_map/dot_general | solution.py:216
  195.2 4.8 %fusion.10 = f32[256,2048]{1,0:T(8,128)} fusion(bf16[816,2048]{1,0:T(8,128)(2,1)} %collective-permute-done.11, f32[256,272]{0,1:T(8,128)} %fusion.12, bf16[256,2048]{1,0:T(8,128)(2,1)S(1)} %constant_dynamic-update-slice_fusion, f32[256]{0:T(256)S(1)} %add_divide_fusion, f32[256]{0:T(256)S(1)} %pad_maximum_fusion.2, pred[272]{0:T(512)(128)(4,1)S(1)} %iota_compare_fusion.2), kind=kOutput, calls=%fused_computation.17 | convolution fusion | flops 570982400 | bytes 5654800 | tf_op jit(solution)/shard_map/dot_general | solution.py:216
  200.0 27.8 %collective-permute-done.10 = bf16[816,2048]{1,0:T(8,128)(2,1)} collective-permute-done((bf16[816,2048]{1,0:T(8,128)(2,1)}, bf16[816,2048]{1,0:T(8,128)(2,1)}, u32[]{:S(2)}, u32[]{:S(2)}) %collective-permute-start.10) | collective-permute-done | bytes 3342368 | tf_op jit(solution)/shard_map/ppermute | solution.py:25
  227.8 2.4 fusion.17
  230.2 4.2 %convolution_add_fusion.1 = f32[256,2048]{1,0:T(8,128)S(1)} fusion(f32[256,2048]{1,0:T(8,128)} %fusion.34, bf16[816,2048]{1,0:T(8,128)(2,1)} %collective-permute-done.9, f32[256,272]{0,1:T(8,128)} %fusion.22, bf16[256,2048]{1,0:T(8,128)(2,1)S(1)} %constant_dynamic-update-slice_fusion, f32[256]{0:T(256)S(1)} %add_divide_fusion, ...), kind=kOutput, calls=%fused_computation.4 | convolution fusion | flops 571506688 | bytes 7751952 | tf_op jit(solution)/shard_map/dot_general | solution.py:216
  234.4 5.5 %fusion.1 = f32[256,2048]{1,0:T(8,128)} fusion(f32[256,2048]{1,0:T(8,128)} %fusion.10, f32[256,2048]{1,0:T(8,128)S(1)} %convolution_add_fusion.1, bf16[816,2048]{1,0:T(8,128)(2,1)} %collective-permute-done.10, f32[256,272]{0,1:T(8,128)} %fusion.17, bf16[256,2048]{1,0:T(8,128)(2,1)S(1)} %constant_dynamic-update-slice_fusion, f32[256]{0:T(256)S(1)} %add_divide_fusion, ...), kind=kOutput, calls=%fused_computation.3 | convolution fusion | flops 572030976 | bytes 9849104 | tf_op jit(solution)/shard_map/dot_general | solution.py:216
  239.8 1.3 slice.148
  241.1 22.8 %collective-permute-start.12 = (bf16[128,2048]{1,0:T(8,128)(2,1)S(1)}, bf16[128,2048]{1,0:T(8,128)(2,1)S(1)}, u32[]{:S(2)}, u32[]{:S(2)}) collective-permute-start(bf16[128,2048]{1,0:T(8,128)(2,1)S(1)} %slice.148), channel_id=1, source_target_pairs={{0,1},{1,0},{2,3},{3,2},{4,5},{5,4},{6,7},{7,6},{8,9},{9,8},{10,11... | collective-permute-start | bytes 1572872 | tf_op jit(solution)/shard_map/ppermute | solution.py:219
  263.9 1.5 collective-permute-done.12
  265.4 1.3 fusion.40
  266.8 33.6 %all_to_all.10 = bf16[16,8,2048]{2,1,0:T(8,128)(2,1)S(1)} all-to-all(bf16[16,8,2048]{2,1,0:T(8,128)(2,1)S(1)} %fusion.40), channel_id=1, replica_groups=mesh['grp'=2,'ep_0'=16,'ep_1'=4,'tp'=2] {'ep_0'}, dimensions={0} | all-to-all | bytes 1048576 | tf_op jit(solution)/shard_map/all_to_all | solution.py:221
  300.5 0.6 add_convert_fusion.2
  (115 shorter events, 2.0 us)
Async XLA Ops:
  7.2 84.2 %copy-start = (bf16[2048,64]{0,1:T(8,128)(2,1)S(1)}, bf16[2048,64]{0,1:T(8,128)(2,1)}, u32[]{:S(2)}) copy-start(bf16[2048,64]{0,1:T(8,128)(2,1)} %param.38) | copy-start | bytes 786436
  7.2 12.8 %copy-start.12 = (bf16[1024,32]{0,1:T(8,128)(2,1)S(1)}, bf16[1024,32]{0,1:T(8,128)(2,1)}, u32[]{:S(2)}) copy-start(bf16[1024,32]{0,1:T(8,128)(2,1)} %param.34) | copy-start | bytes 196612
  7.2 12.5 %copy-start.25 = (s32[16,2]{0,1:T(2,128)S(1)}, s32[16,2]{0,1:T(2,128)}, u32[]{:S(2)}) copy-start(s32[16,2]{0,1:T(2,128)} %param.27) | copy-start | bytes 388
  7.2 12.5 %copy-start.7 = (bf16[16,2048]{1,0:T(8,128)(2,1)S(1)}, bf16[16,2048]{1,0:T(8,128)(2,1)}, u32[]{:S(2)}) copy-start(bf16[16,2048]{1,0:T(8,128)(2,1)} %param.25) | copy-start | bytes 196612
  7.2 12.7 %copy-start.19 = (f32[2048]{0:T(1024)S(1)}, f32[2048]{0:T(1024)}, u32[]{:S(2)}) copy-start(f32[2048]{0:T(1024)} %param.29) | copy-start | bytes 24580
  7.2 12.7 %copy-start.24 = (bf16[16,2]{0,1:T(2,128)(2,1)S(1)}, bf16[16,2]{0,1:T(2,128)(2,1)}, u32[]{:S(2)}) copy-start(bf16[16,2]{0,1:T(2,128)(2,1)} %param.28) | copy-start | bytes 196
  7.2 18.2 %copy-start.13 = (bf16[2048,44]{0,1:T(8,128)(2,1)S(1)}, bf16[2048,44]{0,1:T(8,128)(2,1)}, u32[]{:S(2)}) copy-start(bf16[2048,44]{0,1:T(8,128)(2,1)} %param.46) | copy-start | bytes 540676
  7.3 135.2 %all-gather.2.cloned.1.call-start = ((), (), s32[]{:S(2)}) async-start(), calls=%async_computation.2 | async-start | bytes 4456448 | tf_op jit(solution)/shard_map/all_gather | solution.py:120
  8.3 72.3 %collective-permute-start = (bf16[3,32,1024]{2,1,0:T(8,128)(2,1)S(1)}, bf16[3,32,1024]{2,1,0:T(8,128)(2,1)S(1)}, u32[]{:S(2)}, u32[]{:S(2)}) collective-permute-start(bf16[3,32,1024]{2,1,0:T(8,128)(2,1)S(1)} %pad_maximum_fusion), channel_id=1, source_target_pairs={{2,0},{4,2},{6,4},{0,6},{3,1},{5,3},{7,5},{1,7},{10,8},{12,10},{14... | collective-permute-start | bytes 589832 | tf_op jit(solution)/shard_map/ppermute | solution.py:25
  12.1 68.6 %collective-permute-start.1 = (bf16[3,32,1024]{2,1,0:T(8,128)(2,1)S(1)}, bf16[3,32,1024]{2,1,0:T(8,128)(2,1)S(1)}, u32[]{:S(2)}, u32[]{:S(2)}) collective-permute-start(bf16[3,32,1024]{2,1,0:T(8,128)(2,1)S(1)} %pad_maximum_fusion), channel_id=1, source_target_pairs={{4,0},{6,2},{0,4},{2,6},{5,1},{7,3},{1,5},{3,7},{12,8},{14,10},{8,... | collective-permute-start | bytes 589832 | tf_op jit(solution)/shard_map/ppermute | solution.py:25
  12.4 68.3 %collective-permute-start.2 = (bf16[3,32,1024]{2,1,0:T(8,128)(2,1)S(1)}, bf16[3,32,1024]{2,1,0:T(8,128)(2,1)S(1)}, u32[]{:S(2)}, u32[]{:S(2)}) collective-permute-start(bf16[3,32,1024]{2,1,0:T(8,128)(2,1)S(1)} %pad_maximum_fusion), channel_id=1, source_target_pairs={{6,0},{0,2},{2,4},{4,6},{7,1},{1,3},{3,5},{5,7},{14,8},{8,10},{10,... | collective-permute-start | bytes 589832 | tf_op jit(solution)/shard_map/ppermute | solution.py:25
  13.1 6.9 %collective-permute-start.4 = (bf16[32,1024]{1,0:T(8,128)(2,1)}, bf16[32,1024]{1,0:T(8,128)(2,1)S(1)}, u32[]{:S(2)}, u32[]{:S(2)}) collective-permute-start(bf16[32,1024]{1,0:T(8,128)(2,1)} %bitcast.117), channel_id=1, source_target_pairs={{2,0},{4,2},{6,4},{0,6},{3,1},{5,3},{7,5},{1,7},{10,8},{12,10},{14... | collective-permute-start | bytes 196616 | tf_op jit(solution)/shard_map/ppermute | solution.py:25
  15.1 5.9 %collective-permute-start.5 = (bf16[32,1024]{1,0:T(8,128)(2,1)}, bf16[32,1024]{1,0:T(8,128)(2,1)S(1)}, u32[]{:S(2)}, u32[]{:S(2)}) collective-permute-start(bf16[32,1024]{1,0:T(8,128)(2,1)} %bitcast.118), channel_id=1, source_target_pairs={{4,0},{6,2},{0,4},{2,6},{5,1},{7,3},{1,5},{3,7},{12,8},{14,10},{8,... | collective-permute-start | bytes 196616 | tf_op jit(solution)/shard_map/ppermute | solution.py:25
  17.4 8.8 %copy-start.3 = (bf16[2048,224]{0,1:T(8,128)(2,1)S(1)}, bf16[2048,224]{0,1:T(8,128)(2,1)}, u32[]{:S(2)}) copy-start(bf16[2048,224]{0,1:T(8,128)(2,1)} %param.44) | copy-start | bytes 2752516
  20.0 4.4 %collective-permute-start.6 = (bf16[32,1024]{1,0:T(8,128)(2,1)S(1)}, bf16[32,1024]{1,0:T(8,128)(2,1)S(1)}, u32[]{:S(2)}, u32[]{:S(2)}) collective-permute-start(bf16[32,1024]{1,0:T(8,128)(2,1)S(1)} %bitcast.119), channel_id=1, source_target_pairs={{6,0},{0,2},{2,4},{4,6},{7,1},{1,3},{3,5},{5,7},{14,8},{8,10},{10,... | collective-permute-start | bytes 196616 | tf_op jit(solution)/shard_map/ppermute | solution.py:25
  24.5 56.1 %copy-start.8 = (bf16[1024,32]{0,1:T(8,128)(2,1)S(1)}, bf16[1024,32]{0,1:T(8,128)(2,1)}, u32[]{:S(2)}) copy-start(bf16[1024,32]{0,1:T(8,128)(2,1)} %param.33) | copy-start | bytes 196612
  24.5 56.1 %copy-start.9 = (bf16[1024,32]{0,1:T(8,128)(2,1)S(1)}, bf16[1024,32]{0,1:T(8,128)(2,1)}, u32[]{:S(2)}) copy-start(bf16[1024,32]{0,1:T(8,128)(2,1)} %param.32) | copy-start | bytes 196612
  24.5 56.1 %copy-start.10 = (bf16[1024,32]{0,1:T(8,128)(2,1)S(1)}, bf16[1024,32]{0,1:T(8,128)(2,1)}, u32[]{:S(2)}) copy-start(bf16[1024,32]{0,1:T(8,128)(2,1)} %param.31) | copy-start | bytes 196612
  80.8 5.3 %copy-start.14 = (bf16[2048,44]{0,1:T(8,128)(2,1)S(1)}, bf16[2048,44]{0,1:T(8,128)(2,1)}, u32[]{:S(2)}) copy-start(bf16[2048,44]{0,1:T(8,128)(2,1)} %param.47) | copy-start | bytes 540676
  80.8 6.1 %copy-start.5 = (bf16[224,2048]{1,0:T(8,128)(2,1)S(1)}, bf16[224,2048]{1,0:T(8,128)(2,1)}, u32[]{:S(2)}) copy-start(bf16[224,2048]{1,0:T(8,128)(2,1)} %param.45) | copy-start | bytes 2752516
  80.9 7.0 %copy-start.15 = (bf16[44,2048]{1,0:T(8,128)(2,1)S(1)}, bf16[44,2048]{1,0:T(8,128)(2,1)}, u32[]{:S(2)}) copy-start(bf16[44,2048]{1,0:T(8,128)(2,1)} %param.48) | copy-start | bytes 540676
  80.9 10.4 %copy-start.26 = (bf16[64,1024]{1,0:T(8,128)(2,1)S(1)}, bf16[64,1024]{1,0:T(8,128)(2,1)}, u32[]{:S(2)}) copy-start(bf16[64,1024]{1,0:T(8,128)(2,1)} %param.39) | copy-start | bytes 393220
  80.9 10.4 %copy-start.27 = (f32[1024]{0:T(1024)S(1)}, f32[1024]{0:T(1024)}, u32[]{:S(2)}) copy-start(f32[1024]{0:T(1024)} %param.40) | copy-start | bytes 12292
  82.1 17.9 %all-to-all-start = ((bf16[16,16,384]{2,1,0:T(8,128)(2,1)}), bf16[16,16,384]{2,1,0:T(8,128)(2,1)S(1)}, u32[]{:S(2)}, u32[]{:S(2)}) async-start(bf16[16,16,384]{2,1,0:T(8,128)(2,1)} %bitcast.21), calls=%async_computation | async-start | bytes 393216 | tf_op jit(solution)/shard_map/all_to_all | solution.py:154
  86.9 22.1 %copy-start.11 = (bf16[2048,64]{0,1:T(8,128)(2,1)S(1)}, bf16[2048,64]{0,1:T(8,128)(2,1)}, u32[]{:S(2)}) copy-start(bf16[2048,64]{0,1:T(8,128)(2,1)} %param.35) | copy-start | bytes 786436
  86.9 22.1 %copy-start.17 = (bf16[64,1024]{1,0:T(8,128)(2,1)S(1)}, bf16[64,1024]{1,0:T(8,128)(2,1)}, u32[]{:S(2)}) copy-start(bf16[64,1024]{1,0:T(8,128)(2,1)} %param.36) | copy-start | bytes 393220
  86.9 22.1 %copy-start.21 = (f32[1024]{0:T(1024)S(1)}, f32[1024]{0:T(1024)}, u32[]{:S(2)}) copy-start(f32[1024]{0:T(1024)} %param.37) | copy-start | bytes 12292
  87.9 21.7 %copy-start.22 = (f32[1024]{0:T(1024)S(1)}, f32[1024]{0:T(1024)}, u32[]{:S(2)}) copy-start(f32[1024]{0:T(1024)} %param.41) | copy-start | bytes 12292
  87.9 21.8 %copy-start.23 = (bf16[2048]{0:T(1024)(128)(2,1)S(1)}, bf16[2048]{0:T(1024)(128)(2,1)}, u32[]{:S(2)}) copy-start(bf16[2048]{0:T(1024)(128)(2,1)} %param.49) | copy-start | bytes 12292
  88.7 97.3 %collective-permute-start.11 = (bf16[816,2048]{1,0:T(8,128)(2,1)}, bf16[816,2048]{1,0:T(8,128)(2,1)}, u32[]{:S(2)}, u32[]{:S(2)}) collective-permute-start(bf16[816,2048]{1,0:T(8,128)(2,1)} %get-tuple-element.14), channel_id=1, source_target_pairs={{6,0},{0,2},{2,4},{4,6},{7,1},{1,3},{3,5},{5,7},{14,8},{8,10},{10,... | collective-permute-start | bytes 10027016 | tf_op jit(solution)/shard_map/ppermute | solution.py:25
  88.7 99.9 %collective-permute-start.9 = (bf16[816,2048]{1,0:T(8,128)(2,1)}, bf16[816,2048]{1,0:T(8,128)(2,1)}, u32[]{:S(2)}, u32[]{:S(2)}) collective-permute-start(bf16[816,2048]{1,0:T(8,128)(2,1)} %get-tuple-element.14), channel_id=1, source_target_pairs={{2,0},{4,2},{6,4},{0,6},{3,1},{5,3},{7,5},{1,7},{10,8},{12,10},{14... | collective-permute-start | bytes 10027016 | tf_op jit(solution)/shard_map/ppermute | solution.py:25
  91.3 136.4 %collective-permute-start.10 = (bf16[816,2048]{1,0:T(8,128)(2,1)}, bf16[816,2048]{1,0:T(8,128)(2,1)}, u32[]{:S(2)}, u32[]{:S(2)}) collective-permute-start(bf16[816,2048]{1,0:T(8,128)(2,1)} %get-tuple-element.14), channel_id=1, source_target_pairs={{4,0},{6,2},{0,4},{2,6},{5,1},{7,3},{1,5},{3,7},{12,8},{14,10},{8,... | collective-permute-start | bytes 10027016 | tf_op jit(solution)/shard_map/ppermute | solution.py:25
  100.3 9.6 %collective-permute-start.3 = (bf16[3,16,1024]{2,1,0:T(8,128)(2,1)S(1)}, bf16[3,16,1024]{2,1,0:T(8,128)(2,1)S(1)}, u32[]{:S(2)}, u32[]{:S(2)}) collective-permute-start(bf16[3,16,1024]{2,1,0:T(8,128)(2,1)S(1)} %constant_dynamic-slice_fusion.1), channel_id=1, source_target_pairs={{0,1},{1,0},{2,3},{3,2},{4,5},{5,4},{6,7},{7,6},{8,9},{9,8},{10,11... | collective-permute-start | bytes 294920 | tf_op jit(solution)/shard_map/ppermute | solution.py:160
  134.8 6.6 %copy-start.1 = (f32[16,16,64,64]{3,2,1,0:T(8,128)}, f32[16,16,64,64]{3,2,1,0:T(8,128)S(1)}, u32[]{:S(2)}) copy-start(f32[16,16,64,64]{3,2,1,0:T(8,128)S(1)} %multiply_add_fusion) | copy-start | bytes 12582916
  134.8 7.0 %copy-start.18 = (f32[16,64]{1,0:T(8,128)S(1)}, f32[16,64]{1,0:T(8,128)}, u32[]{:S(2)}) copy-start(f32[16,64]{1,0:T(8,128)} %param.42) | copy-start | bytes 12292
  142.4 4.9 %copy-start.20 = (f32[2048]{0:T(1024)S(1)}, f32[2048]{0:T(1024)}, u32[]{:S(2)}) copy-start(f32[2048]{0:T(1024)} %param.30) | copy-start | bytes 24580
  145.8 38.0 %copy-start.2 = (bf16[2048,224]{0,1:T(8,128)(2,1)S(1)}, bf16[2048,224]{0,1:T(8,128)(2,1)}, u32[]{:S(2)}) copy-start(bf16[2048,224]{0,1:T(8,128)(2,1)} %param.43) | copy-start | bytes 2752516
  145.8 1.3 collective-permute-start.7
  176.0 6.4 %collective-permute-start.8 = (bf16[128,2048]{1,0:T(8,128)(2,1)S(1)}, bf16[128,2048]{1,0:T(8,128)(2,1)}, u32[]{:S(2)}, u32[]{:S(2)}) collective-permute-start(bf16[128,2048]{1,0:T(8,128)(2,1)S(1)} %all_gather.11), channel_id=1, source_target_pairs={{0,1},{1,0},{2,3},{3,2},{4,5},{5,4},{6,7},{7,6},{8,9},{9,8},{10,11... | collective-permute-start | bytes 1572872 | tf_op jit(solution)/shard_map/ppermute | solution.py:193
  186.0 5.1 %copy-start.4 = (bf16[2048,224]{0,1:T(8,128)(2,1)S(1)}, bf16[2048,224]{0,1:T(8,128)(2,1)}, u32[]{:S(2)}) copy-start(bf16[2048,224]{0,1:T(8,128)(2,1)} %param.44) | copy-start | bytes 2752516
  186.0 5.1 %copy-start.6 = (bf16[224,2048]{1,0:T(8,128)(2,1)S(1)}, bf16[224,2048]{1,0:T(8,128)(2,1)}, u32[]{:S(2)}) copy-start(bf16[224,2048]{1,0:T(8,128)(2,1)} %param.45) | copy-start | bytes 2752516
  186.0 5.1 %copy-start.16 = (bf16[48,2048]{1,0:T(8,128)(2,1)S(1)}, bf16[48,2048]{1,0:T(8,128)(2,1)}, u32[]{:S(2)}) copy-start(bf16[48,2048]{1,0:T(8,128)(2,1)} %get-tuple-element.9) | copy-start | bytes 589828
  241.1 24.3 %collective-permute-start.12 = (bf16[128,2048]{1,0:T(8,128)(2,1)S(1)}, bf16[128,2048]{1,0:T(8,128)(2,1)S(1)}, u32[]{:S(2)}, u32[]{:S(2)}) collective-permute-start(bf16[128,2048]{1,0:T(8,128)(2,1)S(1)} %slice.148), channel_id=1, source_target_pairs={{0,1},{1,0},{2,3},{3,2},{4,5},{5,4},{6,7},{7,6},{8,9},{9,8},{10,11... | collective-permute-start | bytes 1572872 | tf_op jit(solution)/shard_map/ppermute | solution.py:219
Sparse Core Ops, SparseCore 0:
  25.5 94.8 all-gather.1

commit v2 on v1

v2 whole, which is shorter than its diff:
```python
import jax
import jax.numpy as jnp
from jax.experimental import pallas as pl
from jax.experimental.pallas import tpu as pltpu
from jax import lax
from jax.sharding import Mesh
from jax.sharding import PartitionSpec as P


LANE_WIDTH = 64
FF_E = 7168
EP = ("ep_0", "ep_1")
GRP_EP = ("grp", "ep_0", "ep_1")
EP_TP = ("ep_0", "ep_1", "tp")
GRP_EP_TP = ("grp", "ep_0", "ep_1", "tp")


RMS_EPS = 1e-06
GROUP_EPS = 0.00064
BF16 = jnp.bfloat16
F32 = jnp.float32


def from_ahead(value, axis, steps):
    size = lax.axis_size(axis)
    return lax.ppermute(value, axis, [((i + steps) % size, i) for i in range(size)])


def in_row_order(pieces, axis):
    count = len(pieces)
    start = (count - lax.axis_index(axis)) % count
    twice = jnp.stack(pieces + pieces[:-1])
    return lax.dynamic_slice_in_dim(twice, start, count, 0)


def rms_norm(values, norm_gain):
    mean_sq = jnp.mean(values * values, axis=-1, keepdims=True)
    return values * lax.rsqrt(mean_sq + RMS_EPS) * norm_gain


def evolve_kernel(
    memory_ref, unit_ref, erase_ref, write_ref, decay_ref, query_ref, value_ref, scaling_ref, bonus_ref,
    after_ref, attended_ref, readout_ref,
):
    heads = memory_ref.shape[1]
    for h in range(heads):
        memory = memory_ref[0, h]
        removal = jnp.sum(memory * unit_ref[0, h : h + 1, :], axis=-1, keepdims=True)
        after = (
            memory * decay_ref[0, h : h + 1, :]
            - removal * erase_ref[0, h : h + 1, :]
            + value_ref[0, :, h : h + 1] * write_ref[0, h : h + 1, :]
        )
        after_ref[0, h] = after
        readout_ref[:, h : h + 1] = jnp.sum(
            after * query_ref[0, h : h + 1, :], axis=-1, keepdims=True
        )
    readout = readout_ref[...]
    centred = readout - jnp.mean(readout, axis=0, keepdims=True)
    spread = jnp.mean(centred * centred, axis=0, keepdims=True)
    attended_ref[0] = (
        centred * lax.rsqrt(spread + GROUP_EPS) * scaling_ref[...] + bonus_ref[0] * value_ref[0]
    )


def evolve_memory(memory, query, key, value, decay, rate, scaling, reward):
    rows, heads, width, _ = memory.shape
    unit = key * lax.rsqrt(jnp.sum(key * key, axis=-1, keepdims=True) + 1.0)
    write = key * rate
    bonus = jnp.sum(query * write * reward, axis=-1)[:, None, :]
    lanes = pl.BlockSpec((1, heads, width), lambda i: (i, 0, 0))
    turned = pl.BlockSpec((1, width, heads), lambda i: (i, 0, 0))
    state = pl.BlockSpec((1, heads, width, width), lambda i: (i, 0, 0, 0))
    after, attended = pl.pallas_call(
        evolve_kernel,
        grid=(rows,),
        in_specs=[
            state, lanes, lanes, lanes, lanes, lanes, turned,
            pl.BlockSpec((width, heads), lambda i: (0, 0)),
            pl.BlockSpec((1, 1, heads), lambda i: (i, 0, 0)),
        ],
        out_specs=[state, turned],
        out_shape=[
            jax.ShapeDtypeStruct(memory.shape, F32),
            jax.ShapeDtypeStruct((rows, width, heads), F32),
        ],
        scratch_shapes=[pltpu.VMEM((width, heads), F32)],
        name="evolve",
    )(memory, unit, unit * rate, write, decay, query, jnp.swapaxes(value, 1, 2), scaling.T, bonus)
    return after, jnp.swapaxes(attended, 1, 2)


def rows_dot(left, right_rows):
    return lax.dot_general(left, right_rows, (((1,), (1,)), ((), ())), preferred_element_type=F32)


def ffn_kernel(pieces, wide, slim, own_ref, other_ref, share_ref, switch_ref, *refs):
    weights, (kept_ref, sent_ref, held, tokens, total, sems) = refs[: 4 * pieces], refs[4 * pieces :]
    block = wide + slim
    copies = []
    for p in range(pieces):
        gate, up, down, common = weights[4 * p : 4 * p + 4]
        parts = []
        for k, ref in enumerate((gate, up, down)):
            parts.append((ref, held.at[p, pl.ds(k * block, wide)]))
            parts.append((common.at[pl.ds(k * slim, slim)], held.at[p, pl.ds(k * block + wide, slim)]))
        copies.append([pltpu.make_async_copy(a, b, sems.at[p, n]) for n, (a, b) in enumerate(parts)])
    for group in copies:
        for copy in group:
            copy.start()
    half = own_ref.shape[0]
    tokens[:half] = own_ref[...]
    tokens[half:] = other_ref[...]
    every = tokens[...]
    share = share_ref[...]
    branch = jax.nn.sigmoid(rows_dot(switch_ref[...], every)[:1])
    for p in range(pieces):
        for copy in copies[p]:
            copy.wait()
        both = rows_dot(held[p, : 2 * block], every)
        gate_val, up_val = both[:block], both[block:]
        row = lax.broadcasted_iota(jnp.int32, (block, 1), 0)
        scale = jnp.where(row < wide, share, branch)
        hidden = (gate_val * jax.nn.sigmoid(gate_val) * up_val * scale).astype(BF16)
        term = lax.dot_general(
            hidden, held[p, 2 * block :], (((0,), (0,)), ((), ())), preferred_element_type=F32
        )
        if p == 0:
            total[...] = term
        elif p < pieces - 1:
            total[...] += term
        else:
            term = total[...] + term
            kept_ref[...] = term[:half]
            sent_ref[...] = term[half:].astype(BF16)


def ffn(own_in, other_in, share, switch, pieces):
    half, width = own_in.shape
    wide, slim = pieces[0][0].shape[0], pieces[0][3].shape[0] // 3
    count = len(pieces)
    vmem = pl.BlockSpec(memory_space=pltpu.VMEM)
    hbm = pl.BlockSpec(memory_space=pl.ANY)
    return pl.pallas_call(
        lambda *refs: ffn_kernel(count, wide, slim, *refs),
        in_specs=[vmem] * 4 + [hbm] * (4 * count),
        out_specs=[vmem, vmem],
        out_shape=[
            jax.ShapeDtypeStruct((half, width), F32),
            jax.ShapeDtypeStruct((half, width), BF16),
        ],
        scratch_shapes=[
            pltpu.VMEM((count, 3 * (wide + slim), width), BF16),
            pltpu.VMEM((2 * half, width), BF16),
            pltpu.VMEM((2 * half, width), F32),
            pltpu.SemaphoreType.DMA((count, 6)),
        ],
        compiler_params=pltpu.CompilerParams(vmem_limit_bytes=48 * 1024 * 1024),
        name="ffn",
    )(own_in, other_in, share, switch, *[ref for piece in pieces for ref in piece])


def body(
    fresh_inputs,
    memory_arrays,
    chosen_specialist,
    chosen_coefficient,
    first_rescale,
    second_rescale,
    receiver_projector,
    address_projector,
    content_projector,
    final_projector,
    forget_narrowing,
    forget_widening,
    forget_bias,
    learning_narrowing,
    learning_widening,
    learning_bias,
    lane_scaling,
    instant_reward,
    specialist_switch,
    specialist_expand,
    specialist_contract,
    common_activator,
    common_expand,
    common_contract,
    common_switch,
):
    own_rows, model_width = fresh_inputs.shape
    tp_count = lax.axis_size("tp")
    tp_rank = lax.axis_index("tp")
    z_count = lax.axis_size("ep_0")
    x_count = lax.axis_size("ep_1")
    half_width = model_width // tp_count
    head_count = half_width // LANE_WIDTH
    half_rows = own_rows // tp_count
    swap = [(0, 1), (1, 0)]

    def pick(value, rank, width, dim):
        return lax.dynamic_slice_in_dim(value, rank * width, width, dim)

    projector_rows = jnp.stack(
        (receiver_projector.T, address_projector.T, content_projector.T, final_projector.T)
    )
    projector_row = in_row_order(
        [projector_rows] + [from_ahead(projector_rows, "ep_1", k) for k in range(1, x_count)], "ep_1"
    )
    qkv_row = jnp.swapaxes(projector_row[:, :3], 0, 1).reshape(-1, half_width)
    final_row = projector_row[:, 3].reshape(-1, half_width)

    expert_cols = specialist_switch.shape[1]
    pad = ((0, -common_activator.shape[1] % 16), (0, 0))
    common = jnp.concatenate(
        [jnp.pad(w, pad) for w in (common_activator.T, common_expand.T, common_contract)]
    )
    own_piece = [specialist_switch.T, specialist_expand.T, specialist_contract, common]
    ahead, behind, across = [], [], []
    for w in own_piece:
        ahead.append(from_ahead(w, "ep_1", 1))
        behind.append(from_ahead(w, "ep_1", x_count - 1))
    for k in range(len(own_piece)):
        if k % 2 == 0:
            across.append(from_ahead(ahead[k], "ep_1", 1))
        else:
            across.append(from_ahead(behind[k], "ep_1", x_count - 1))
    pieces = [own_piece, ahead, behind, across]

    names = lax.broadcasted_iota(jnp.int32, (own_rows, 128), 1)
    share_table = jnp.zeros((own_rows, 128), F32)
    for k in range(chosen_specialist.shape[1]):
        share_table += jnp.where(
            chosen_specialist[:, k : k + 1] == names, chosen_coefficient[:, k : k + 1].astype(F32), 0.0
        )
    ring_own = jnp.concatenate((fresh_inputs, share_table.astype(BF16)), axis=1)
    ring_own = pick(ring_own, tp_rank, half_rows, 0)
    ring = lax.all_gather(ring_own, "ep_0", axis=0, tiled=True)
    ring_rows = ring.shape[0]
    ring_share = ring[:, model_width:]
    ring_fresh = ring[:, :model_width].astype(F32)
    ring_normed = rms_norm(ring_fresh, first_rescale).astype(BF16)
    give = jnp.concatenate((pick(ring_normed, 1 - tp_rank, half_width, 1), ring_share), axis=1)
    got = lax.ppermute(give, "tp", swap)
    other_share = got[:, half_width:]
    mine = pick(ring_normed, tp_rank, half_width, 1).reshape(z_count, 1, half_rows, half_width)
    theirs = got[:, :half_width].reshape(z_count, 1, half_rows, half_width)
    first = tp_rank == 0
    ring_half = jnp.concatenate(
        (jnp.where(first, mine, theirs), jnp.where(first, theirs, mine)), axis=1
    ).reshape(z_count * own_rows, half_width)

    partial = rows_dot(ring_half, qkv_row).astype(BF16)
    partial = lax.all_to_all(
        partial.reshape(z_count, own_rows, -1), "ep_0", 0, 0, tiled=True
    ).reshape(z_count, own_rows, 3, -1)
    partial = jnp.transpose(partial, (2, 1, 0, 3)).reshape(3, own_rows, model_width)
    got = lax.ppermute(pick(partial, 1 - tp_rank, half_width, 2), "tp", swap)
    projected = (pick(partial, tp_rank, half_width, 2).astype(F32) + got.astype(F32)).astype(BF16)

    def divide_lanes(channels):
        return channels.astype(F32).reshape(own_rows, head_count, LANE_WIDTH)

    normed = rms_norm(fresh_inputs.astype(F32), first_rescale).astype(BF16)
    decay_mid = jnp.tanh(
        jnp.dot(normed, forget_narrowing, preferred_element_type=F32)
    ).astype(BF16)
    decay_pre = forget_bias + jnp.dot(decay_mid, forget_widening, preferred_element_type=F32)
    decay_vals = jnp.exp(-jnp.exp(-jax.nn.softplus(-decay_pre) - 0.5))
    rate_mid = jnp.dot(normed, learning_narrowing, preferred_element_type=F32).astype(BF16)
    rate_vals = jax.nn.sigmoid(
        learning_bias + jnp.dot(rate_mid, learning_widening, preferred_element_type=F32)
    )
    memory_after, memory_retrieval = evolve_memory(
        memory_arrays,
        divide_lanes(projected[0]),
        divide_lanes(projected[1]),
        divide_lanes(projected[2]),
        divide_lanes(decay_vals),
        divide_lanes(rate_vals),
        lane_scaling.reshape(head_count, LANE_WIDTH),
        instant_reward,
    )
    attended = memory_retrieval.reshape(own_rows, half_width).astype(BF16)
    ring_attended = lax.all_gather(attended, "ep_0", axis=0, tiled=True)
    out_part = rows_dot(ring_attended, final_row).astype(BF16)
    out_part = out_part.reshape(z_count, own_rows, -1)
    got = lax.ppermute(pick(out_part, 1 - tp_rank, half_rows, 1), "tp", swap)
    mixed = (pick(out_part, tp_rank, half_rows, 1).astype(F32) + got.astype(F32)).astype(BF16)
    mixed = mixed.reshape(1, ring_rows, -1)
    mixed = lax.all_gather(mixed, "ep_0", axis=0, tiled=True)
    mixed = jnp.swapaxes(mixed, 0, 1).reshape(ring_rows, model_width)
    residual = ring_fresh + mixed.astype(F32)
    ring_in = rms_norm(residual, second_rescale).astype(BF16)
    other_in = lax.ppermute(ring_in, "tp", swap)

    flat_rank = lax.axis_index(EP) * tp_count + tp_rank
    expert = flat_rank * expert_cols // FF_E
    share = jnp.concatenate((ring_share, other_share)).astype(F32)
    lane = lax.broadcasted_iota(jnp.int32, share.shape, 1)
    expert_share = jnp.sum(jnp.where(lane == expert, share, 0.0), axis=1)[None, :]
    switch = jnp.broadcast_to(common_switch[None, :], (16, model_width))
    kept, sent = ffn(ring_in, other_in, expert_share, switch, pieces)
    got = lax.ppermute(sent, "tp", swap)
    ring_total = (kept + got.astype(F32)).astype(BF16)
    blocks = lax.all_to_all(
        ring_total.reshape(z_count, half_rows, model_width), "ep_0", 0, 0, tiled=True
    )
    routed = jnp.sum(blocks.astype(F32), axis=0)
    own_residual = pick(residual, lax.axis_index("ep_0"), half_rows, 0)
    return ((own_residual + routed).astype(BF16), memory_after)


def solution(mesh):
    torus = Mesh(
        mesh.devices.reshape(mesh.shape["grp"], 16, 4, mesh.shape["tp"]),
        ("grp", "ep_0", "ep_1", "tp"),
    )
    return jax.shard_map(
        body,
        mesh=torus,
        in_specs=(
            P(GRP_EP, None),
            P(GRP_EP, "tp", None, None),
            P(GRP_EP, None),
            P(GRP_EP, None),
            P(),
            P(),
            P("tp", EP),
            P("tp", EP),
            P("tp", EP),
            P("tp", EP),
            P(),
            P(None, "tp"),
            P("tp"),
            P(),
            P(None, "tp"),
            P("tp"),
            P("tp"),
            P("tp", None),
            P(None, EP_TP),
            P(None, EP_TP),
            P(EP_TP, None),
            P(None, EP_TP),
            P(None, EP_TP),
            P(EP_TP, None),
            P(),
        ),
        out_specs=(P(GRP_EP_TP, None), P(GRP_EP, "tp", None, None)),
        check_vma=False,
    )
```

time: 314 us -> 325 us (1.035)
  the two profiles are of different devices: /device:TPU:33 before, /device:TPU:38 now
where the time goes in v2:
time: 325 us; the launch traced here: 324 us
  waiting for transfers between devices  106 us (33%)
  blocking collectives  97.8 us (30%)
  starting transfers between devices  42.8 us (13%)
  Pallas kernels  41.4 us (13%)
  local copies, waits for them, and re-layouts  16.6 us (5%)
  other arithmetic  14.3 us (4%)
  matrix products  4.2 us (1%)
    ppermute x15, waiting for transfers between devices, from_ahead(): lax.ppermute(value, axis, [((i + steps) % size, i) for i in range(size)])  63 us
    all_gather x1, blocking collectives, body(): ring = lax.all_gather(ring_own, 'ep_0', axis=0, tiled=True)  35.9 us
    ppermute x15, starting transfers between devices, from_ahead(): lax.ppermute(value, axis, [((i + steps) % size, i) for i in range(size)])  33.7 us
    all_gather x1, blocking collectives, body(): ring_attended = lax.all_gather(attended, 'ep_0', axis=0, tiled=True)  33.1 us
    all_to_all x1, waiting for transfers between devices, body(): lax.all_to_all(ring_total.reshape(z_count, half_rows, model_width), 'ep_0...  29 us
    all_gather x1, blocking collectives, body(): mixed = lax.all_gather(mixed, 'ep_0', axis=0, tiled=True)  28.8 us
    pallas_call x1, Pallas kernels, evolve_memory(): pl.pallas_call(evolve_kernel, grid=(rows,), in_specs=[state, lanes, lanes...  28 us
    pallas_call x1, Pallas kernels, ffn(): pl.pallas_call(lambda *refs: ffn_kernel(count, wide, slim, *refs), in_spe...  13.4 us
  transfers between devices with their start and end apart: 22, of which 8 were waited for; matrix products, arithmetic and copies ran while one was open for 9% of the time, Pallas kernels for 9%

profile of v2, /device:TPU:38, one launch (start us, length us, event | category | flops | bytes accessed | tf_op | source)
XLA Modules:
  0.0 324.4 jit_solution(15987875852057818677)
XLA Ops:
  0.7 1.7 pad_maximum_fusion.2
  2.4 1.1 collective-permute-start.2
  3.5 18.8 %collective-permute-start.1 = (bf16[4,32,1024]{2,1,0:T(8,128)(2,1)}, bf16[4,32,1024]{2,1,0:T(8,128)(2,1)}, u32[]{:S(2)}, u32[]{:S(2)}) collective-permute-start(bf16[4,32,1024]{2,1,0:T(8,128)(2,1)} %pad_maximum_fusion.2), channel_id=1, source_target_pairs={{2,0},{4,2},{6,4},{0,6},{3,1},{5,3},{7,5},{1,7},{10,8},{12,10},{14... | collective-permute-start | bytes 786440 | tf_op jit(solution)/shard_map/ppermute | solution.py:26
  22.3 1.2 fusion.14.refs_7_
  23.5 1.3 collective-permute-start.14
  24.8 1.0 collective-permute-start.10
  25.8 0.8 slice_bitcast_fusion.1
  26.6 0.7 bitcast_convert_fusion.1
  27.4 0.8 fusion.24
  28.1 35.9 %all_gather.9 = bf16[128,2176]{1,0:T(8,128)(2,1)S(1)} all-gather(bf16[8,2176]{1,0:T(8,128)(2,1)S(1)} %fusion.24), channel_id=1, replica_groups=mesh['grp'=2,'ep_0'=16,'ep_1'=4,'tp'=2] {'ep_0'}, dimensions={0}, use_global_device_ids=true | all-gather | bytes 591872 | tf_op jit(solution)/shard_map/all_gather | solution.py:237
  64.0 0.2 fusion.10
  64.2 0.2 fusion.12
  64.5 0.8 pad_maximum_fusion.1
  65.2 0.7 bitcast_dynamic-update-slice_fusion.3
  65.9 1.7 bitcast_dynamic-update-slice_fusion.1
  67.6 2.2 collective-permute-start.11
  69.9 0.7 bitcast_dynamic-update-slice_fusion.5
  70.6 1.7 bitcast_dynamic-update-slice_fusion
  72.3 0.7 bitcast_dynamic-update-slice_fusion.4
  73.0 1.7 bitcast_dynamic-update-slice_fusion.2
  74.6 0.7 bitcast_dynamic-update-slice_fusion.6
  75.4 1.2 constant_dynamic-slice_fusion
  76.7 0.6 copy-done.12
  77.4 1.1 convolution_convert_fusion
  78.5 4.0 %all-to-all-start = ((bf16[16,16,384]{2,1,0:T(8,128)(2,1)}), bf16[16,16,384]{2,1,0:T(8,128)(2,1)S(1)}, u32[]{:S(2)}, u32[]{:S(2)}) async-start(bf16[16,16,384]{2,1,0:T(8,128)(2,1)} %bitcast.28), calls=%async_computation | async-start | bytes 393216 | tf_op jit(solution)/shard_map/all_to_all | solution.py:253
  82.5 0.1 fusion.16
  82.7 0.7 copy.60
  83.4 0.4 fusion.8
  83.9 1.4 fusion.23
  85.3 0.7 reshape.150.decay_ref
  86.1 12.2 %all-to-all-done = bf16[16,16,384]{2,1,0:T(8,128)(2,1)S(1)} async-done(((bf16[16,16,384]{2,1,0:T(8,128)(2,1)}), bf16[16,16,384]{2,1,0:T(8,128)(2,1)S(1)}, u32[]{:S(2)}, u32[]{:S(2)}) %all-to-all-start) | async-done | bytes 196640 | tf_op jit(solution)/shard_map/all_to_all | solution.py:253
  98.4 0.2 copy.58
  98.7 0.1 collective-permute-start.4
  98.8 1.7 constant_dynamic-slice_fusion.3
  101.0 1.0 copy.59
  102.0 1.4 multiply_reduce_fusion.1
  103.4 28.0 %evolve.1 = (f32[16,16,64,64]{3,2,1,0:T(8,128)}, f32[16,64,16]{2,1,0:T(8,128)}) custom-call(f32[16,16,64,64]{3,2,1,0:T(8,128)} %memory_ref.1, f32[16,16,64]{2,1,0:T(8,128)} %get-tuple-element.19.unit_ref, f32[16,16,64]{2,1,0:T(8,128)} %get-tuple-element.18.erase_ref, f32[16,16,64]{2,1,0:T(8,128)} %get-tuple-element.13.write_ref, ...), custom_call_target="tpu_custom_call" | custom-call | tf_op jit(solution)/shard_map/evolve/pallas_call | solution.py:74
  131.5 1.2 convert_bitcast_fusion.1
  132.6 0.8 copy.61
  133.4 1.0 convert_element_type.136
  134.3 33.1 %all_gather.10 = bf16[256,1024]{1,0:T(8,128)(2,1)S(1)} all-gather(bf16[16,1024]{1,0:T(8,128)(2,1)S(1)} %convert_element_type.136), channel_id=1, replica_groups=mesh['grp'=2,'ep_0'=16,'ep_1'=4,'tp'=2] {'ep_0'}, dimensions={0}, use_global_device_ids=true | all-gather | bytes 557056 | tf_op jit(solution)/shard_map/all_gather | solution.py:284
  167.4 1.3 convolution_convert_fusion.1
  168.7 0.1 collective-permute-start.5
  168.9 0.3 collective-permute-start.7
  169.2 3.2 collective-permute-start.12
  172.4 0.1 collective-permute-start.9
  172.6 28.8 %all_gather.11 = bf16[16,128,128]{2,1,0:T(8,128)(2,1)S(1)} all-gather(bf16[1,128,128]{2,1,0:T(8,128)(2,1)S(1)} %fusion.25), channel_id=1, replica_groups=mesh['grp'=2,'ep_0'=16,'ep_1'=4,'tp'=2] {'ep_0'}, dimensions={0}, use_global_device_ids=true | all-gather | bytes 557056 | tf_op jit(solution)/shard_map/all_gather | solution.py:290
  201.4 3.4 %collective-permute-start.13 = (bf16[224,2048]{1,0:T(8,128)(2,1)S(1)}, bf16[224,2048]{1,0:T(8,128)(2,1)S(1)}, u32[]{:S(2)}, u32[]{:S(2)}) collective-permute-start(bf16[224,2048]{1,0:T(8,128)(2,1)S(1)} %copy-done.5), channel_id=1, source_target_pairs={{6,0},{0,2},{2,4},{4,6},{7,1},{1,3},{3,5},{5,7},{14,8},{8,10},{10,... | collective-permute-start | bytes 2752520 | tf_op jit(solution)/shard_map/ppermute | solution.py:26
  204.8 0.3 multiply_reduce_fusion
  205.1 2.1 collective-permute-start.18
  207.3 6.0 %collective-permute-done.8.refs_9_ = bf16[224,2048]{1,0:T(8,128)(2,1)S(1)} collective-permute-done((bf16[224,2048]{1,0:T(8,128)(2,1)S(1)}, bf16[224,2048]{1,0:T(8,128)(2,1)S(1)}, u32[]{:S(2)}, u32[]{:S(2)}) %collective-permute-start.8) | collective-permute-done | bytes 917536 | tf_op jit(solution)/shard_map/ppermute | solution.py:26
  213.2 19.8 %collective-permute-done.9.refs_10_ = bf16[224,2048]{1,0:T(8,128)(2,1)} collective-permute-done((bf16[224,2048]{1,0:T(8,128)(2,1)}, bf16[224,2048]{1,0:T(8,128)(2,1)}, u32[]{:S(2)}, u32[]{:S(2)}) %collective-permute-start.9) | collective-permute-done | bytes 917536 | tf_op jit(solution)/shard_map/ppermute | solution.py:26
  233.0 0.2 multiply_convert_fusion.refs_0_
  233.2 0.9 copy-done.7
  234.3 4.0 %collective-permute-done.18.refs_19_ = bf16[144,2048]{1,0:T(8,128)(2,1)} collective-permute-done((bf16[144,2048]{1,0:T(8,128)(2,1)}, bf16[144,2048]{1,0:T(8,128)(2,1)}, u32[]{:S(2)}, u32[]{:S(2)}) %collective-permute-start.18) | collective-permute-done | bytes 589856 | tf_op jit(solution)/shard_map/ppermute | solution.py:26
  238.3 14.3 %collective-permute-done.15.refs_16_ = bf16[224,2048]{1,0:T(8,128)(2,1)} collective-permute-done((bf16[224,2048]{1,0:T(8,128)(2,1)}, bf16[224,2048]{1,0:T(8,128)(2,1)}, u32[]{:S(2)}, u32[]{:S(2)}) %collective-permute-start.15) | collective-permute-done | bytes 917536 | tf_op jit(solution)/shard_map/ppermute | solution.py:26
  252.7 18.9 %collective-permute-done.17.refs_18_ = bf16[224,2048]{1,0:T(8,128)(2,1)} collective-permute-done((bf16[224,2048]{1,0:T(8,128)(2,1)}, bf16[224,2048]{1,0:T(8,128)(2,1)}, u32[]{:S(2)}, u32[]{:S(2)}) %collective-permute-start.17) | collective-permute-done | bytes 917536 | tf_op jit(solution)/shard_map/ppermute | solution.py:26
  271.6 13.4 %ffn.1 = (f32[128,2048]{1,0:T(8,128)}, bf16[128,2048]{1,0:T(8,128)(2,1)S(1)}) custom-call(bf16[128,2048]{1,0:T(8,128)(2,1)S(1)} %multiply_convert_fusion.refs_0_, bf16[128,2048]{1,0:T(8,128)(2,1)} %collective-permute-done.6.refs_1_, f32[1,256]{1,0:T(1,128)S(1)} %bitcast.94, bf16[16,2048]{1,0:T(8,128)(2,1)S(1)} %broadcast_in_dim.64.refs_3_, ...), custom_call_target="tpu_custom_call" | custom-call | tf_op jit(solution)/shard_map/ffn/pallas_call | solution.py:144
  284.9 0.1 collective-permute-start.19
  285.1 1.9 collective-permute-done.19
  287.0 2.1 fusion.15
  289.1 4.7 %all-to-all-start.1 = ((bf16[16,8,2048]{2,1,0:T(8,128)(2,1)}), bf16[16,8,2048]{2,1,0:T(8,128)(2,1)S(1)}, u32[]{:S(2)}, u32[]{:S(2)}) async-start(bf16[16,8,2048]{2,1,0:T(8,128)(2,1)} %fusion.15), calls=%async_computation.1 | async-start | bytes 1048576 | tf_op jit(solution)/shard_map/all_to_all | solution.py:305
  293.9 29.0 %all-to-all-done.1 = bf16[16,8,2048]{2,1,0:T(8,128)(2,1)S(1)} async-done(((bf16[16,8,2048]{2,1,0:T(8,128)(2,1)}), bf16[16,8,2048]{2,1,0:T(8,128)(2,1)S(1)}, u32[]{:S(2)}, u32[]{:S(2)}) %all-to-all-start.1) | async-done | bytes 524320 | tf_op jit(solution)/shard_map/all_to_all | solution.py:305
  322.9 1.5 add_convert_fusion.2
  (93 shorter events, 1.4 us)
Async XLA Ops:
  0.6 82.8 %copy-start = (bf16[2048,64]{0,1:T(8,128)(2,1)S(1)}, bf16[2048,64]{0,1:T(8,128)(2,1)}, u32[]{:S(2)}) copy-start(bf16[2048,64]{0,1:T(8,128)(2,1)} %param.38) | copy-start | bytes 786436
  0.6 63.6 %copy-start.14 = (f32[2048]{0:T(1024)S(1)}, f32[2048]{0:T(1024)}, u32[]{:S(2)}) copy-start(f32[2048]{0:T(1024)} %param.29) | copy-start | bytes 24580
  2.4 65.2 %collective-permute-start.2 = (bf16[4,32,1024]{2,1,0:T(8,128)(2,1)}, bf16[4,32,1024]{2,1,0:T(8,128)(2,1)S(1)}, u32[]{:S(2)}, u32[]{:S(2)}) collective-permute-start(bf16[4,32,1024]{2,1,0:T(8,128)(2,1)} %pad_maximum_fusion.2), channel_id=1, source_target_pairs={{4,0},{6,2},{0,4},{2,6},{5,1},{7,3},{1,5},{3,7},{12,8},{14,10},{8,... | collective-permute-start | bytes 786440 | tf_op jit(solution)/shard_map/ppermute | solution.py:26
  3.5 62.4 %collective-permute-start.1 = (bf16[4,32,1024]{2,1,0:T(8,128)(2,1)}, bf16[4,32,1024]{2,1,0:T(8,128)(2,1)}, u32[]{:S(2)}, u32[]{:S(2)}) collective-permute-start(bf16[4,32,1024]{2,1,0:T(8,128)(2,1)} %pad_maximum_fusion.2), channel_id=1, source_target_pairs={{2,0},{4,2},{6,4},{0,6},{3,1},{5,3},{7,5},{1,7},{10,8},{12,10},{14... | collective-permute-start | bytes 786440 | tf_op jit(solution)/shard_map/ppermute | solution.py:26
  22.3 48.3 %collective-permute-start.3 = (bf16[4,32,1024]{2,1,0:T(8,128)(2,1)}, bf16[4,32,1024]{2,1,0:T(8,128)(2,1)}, u32[]{:S(2)}, u32[]{:S(2)}) collective-permute-start(bf16[4,32,1024]{2,1,0:T(8,128)(2,1)} %pad_maximum_fusion.2), channel_id=1, source_target_pairs={{6,0},{0,2},{2,4},{4,6},{7,1},{1,3},{3,5},{5,7},{14,8},{8,10},{10,... | collective-permute-start | bytes 786440 | tf_op jit(solution)/shard_map/ppermute | solution.py:26
  23.5 41.7 %copy-start.8 = (bf16[1024,32]{0,1:T(8,128)(2,1)S(1)}, bf16[1024,32]{0,1:T(8,128)(2,1)}, u32[]{:S(2)}) copy-start(bf16[1024,32]{0,1:T(8,128)(2,1)} %param.34) | copy-start | bytes 196612
  23.5 41.7 %copy-start.9 = (bf16[1024,32]{0,1:T(8,128)(2,1)S(1)}, bf16[1024,32]{0,1:T(8,128)(2,1)}, u32[]{:S(2)}) copy-start(bf16[1024,32]{0,1:T(8,128)(2,1)} %param.33) | copy-start | bytes 196612
  23.5 41.7 %copy-start.10 = (bf16[1024,32]{0,1:T(8,128)(2,1)S(1)}, bf16[1024,32]{0,1:T(8,128)(2,1)}, u32[]{:S(2)}) copy-start(bf16[1024,32]{0,1:T(8,128)(2,1)} %param.32) | copy-start | bytes 196612
  23.5 41.7 %copy-start.11 = (bf16[1024,32]{0,1:T(8,128)(2,1)S(1)}, bf16[1024,32]{0,1:T(8,128)(2,1)}, u32[]{:S(2)}) copy-start(bf16[1024,32]{0,1:T(8,128)(2,1)} %param.31) | copy-start | bytes 196612
  23.5 145.7 %collective-permute-start.14 = (bf16[144,2048]{1,0:T(8,128)(2,1)S(1)}, bf16[144,2048]{1,0:T(8,128)(2,1)}, u32[]{:S(2)}, u32[]{:S(2)}) collective-permute-start(bf16[144,2048]{1,0:T(8,128)(2,1)S(1)} %fusion.14.refs_7_), channel_id=1, source_target_pairs={{6,0},{0,2},{2,4},{4,6},{7,1},{1,3},{3,5},{5,7},{14,8},{8,10},{10,... | collective-permute-start | bytes 1769480 | tf_op jit(solution)/shard_map/ppermute | solution.py:26
  24.8 147.6 %collective-permute-start.10 = (bf16[144,2048]{1,0:T(8,128)(2,1)S(1)}, bf16[144,2048]{1,0:T(8,128)(2,1)}, u32[]{:S(2)}, u32[]{:S(2)}) collective-permute-start(bf16[144,2048]{1,0:T(8,128)(2,1)S(1)} %fusion.14.refs_7_), channel_id=1, source_target_pairs={{2,0},{4,2},{6,4},{0,6},{3,1},{5,3},{7,5},{1,7},{10,8},{12,10},{14... | collective-permute-start | bytes 1769480 | tf_op jit(solution)/shard_map/ppermute | solution.py:26
  64.0 3.6 %copy-start.1 = (bf16[2048,224]{0,1:T(8,128)(2,1)S(1)}, bf16[2048,224]{0,1:T(8,128)(2,1)}, u32[]{:S(2)}) copy-start(bf16[2048,224]{0,1:T(8,128)(2,1)} %param.43) | copy-start | bytes 2752516
  65.9 10.7 %collective-permute-start = (bf16[128,1152]{1,0:T(8,128)(2,1)}, bf16[128,1152]{1,0:T(8,128)(2,1)S(1)}, u32[]{:S(2)}, u32[]{:S(2)}) collective-permute-start(bf16[128,1152]{1,0:T(8,128)(2,1)} %pad_maximum_fusion.1), channel_id=1, source_target_pairs={{0,1},{1,0},{2,3},{3,2},{4,5},{5,4},{6,7},{7,6},{8,9},{9,8},{10,11... | collective-permute-start | bytes 884744 | tf_op jit(solution)/shard_map/ppermute | solution.py:243
  67.6 133.8 %collective-permute-start.11 = (bf16[224,2048]{1,0:T(8,128)(2,1)S(1)}, bf16[224,2048]{1,0:T(8,128)(2,1)}, u32[]{:S(2)}, u32[]{:S(2)}) collective-permute-start(bf16[224,2048]{1,0:T(8,128)(2,1)S(1)} %bitcast.88), channel_id=1, source_target_pairs={{6,0},{0,2},{2,4},{4,6},{7,1},{1,3},{3,5},{5,7},{14,8},{8,10},{10,... | collective-permute-start | bytes 2752520 | tf_op jit(solution)/shard_map/ppermute | solution.py:26
  76.5 5.9 %copy-start.13 = (bf16[16,2048]{1,0:T(8,128)(2,1)S(1)}, bf16[16,2048]{1,0:T(8,128)(2,1)}, u32[]{:S(2)}) copy-start(bf16[16,2048]{1,0:T(8,128)(2,1)} %param.25) | copy-start | bytes 196612
  76.6 6.1 %copy-start.17 = (f32[1024]{0:T(1024)S(1)}, f32[1024]{0:T(1024)}, u32[]{:S(2)}) copy-start(f32[1024]{0:T(1024)} %param.41) | copy-start | bytes 12292
  76.6 6.8 %copy-start.19 = (bf16[64,1024]{1,0:T(8,128)(2,1)S(1)}, bf16[64,1024]{1,0:T(8,128)(2,1)}, u32[]{:S(2)}) copy-start(bf16[64,1024]{1,0:T(8,128)(2,1)} %param.39) | copy-start | bytes 393220
  76.6 6.8 %copy-start.21 = (f32[1024]{0:T(1024)S(1)}, f32[1024]{0:T(1024)}, u32[]{:S(2)}) copy-start(f32[1024]{0:T(1024)} %param.40) | copy-start | bytes 12292
  76.6 0.7 copy-start.12
  77.3 6.6 %copy-start.20 = (bf16[64,1024]{1,0:T(8,128)(2,1)S(1)}, bf16[64,1024]{1,0:T(8,128)(2,1)}, u32[]{:S(2)}) copy-start(bf16[64,1024]{1,0:T(8,128)(2,1)} %param.36) | copy-start | bytes 393220
  77.3 6.6 %copy-start.22 = (f32[1024]{0:T(1024)S(1)}, f32[1024]{0:T(1024)}, u32[]{:S(2)}) copy-start(f32[1024]{0:T(1024)} %param.37) | copy-start | bytes 12292
  78.5 19.8 %all-to-all-start = ((bf16[16,16,384]{2,1,0:T(8,128)(2,1)}), bf16[16,16,384]{2,1,0:T(8,128)(2,1)S(1)}, u32[]{:S(2)}, u32[]{:S(2)}) async-start(bf16[16,16,384]{2,1,0:T(8,128)(2,1)} %bitcast.28), calls=%async_computation | async-start | bytes 393216 | tf_op jit(solution)/shard_map/all_to_all | solution.py:253
  98.4 3.6 %copy-start.15 = (f32[16,64]{1,0:T(8,128)S(1)}, f32[16,64]{1,0:T(8,128)}, u32[]{:S(2)}) copy-start(f32[16,64]{1,0:T(8,128)} %param.42) | copy-start | bytes 12292
  98.7 1.8 collective-permute-start.4
  100.8 2.7 copy-start.4
  131.4 37.7 %copy-start.2 = (bf16[2048,224]{0,1:T(8,128)(2,1)S(1)}, bf16[2048,224]{0,1:T(8,128)(2,1)}, u32[]{:S(2)}) copy-start(bf16[2048,224]{0,1:T(8,128)(2,1)} %param.44) | copy-start | bytes 2752516
  134.3 67.1 %copy-start.5 = (bf16[224,2048]{1,0:T(8,128)(2,1)S(1)}, bf16[224,2048]{1,0:T(8,128)(2,1)}, u32[]{:S(2)}) copy-start(bf16[224,2048]{1,0:T(8,128)(2,1)} %refs_6_.1) | copy-start | bytes 2752516
  167.4 65.6 %copy-start.16 = (f32[2048]{0:T(1024)S(1)}, f32[2048]{0:T(1024)}, u32[]{:S(2)}) copy-start(f32[2048]{0:T(1024)} %param.30) | copy-start | bytes 24580
  168.7 3.7 %collective-permute-start.5 = (bf16[16,8,128]{2,1,0:T(8,128)(2,1)S(1)}, bf16[16,8,128]{2,1,0:T(8,128)(2,1)S(1)}, u32[]{:S(2)}, u32[]{:S(2)}) collective-permute-start(bf16[16,8,128]{2,1,0:T(8,128)(2,1)S(1)} %constant_dynamic-slice_fusion.1), channel_id=1, source_target_pairs={{0,1},{1,0},{2,3},{3,2},{4,5},{5,4},{6,7},{7,6},{8,9},{9,8},{10,11... | collective-permute-start | bytes 98312 | tf_op jit(solution)/shard_map/ppermute | solution.py:287
  168.9 36.3 %collective-permute-start.7 = (bf16[224,2048]{1,0:T(8,128)(2,1)S(1)}, bf16[224,2048]{1,0:T(8,128)(2,1)}, u32[]{:S(2)}, u32[]{:S(2)}) collective-permute-start(bf16[224,2048]{1,0:T(8,128)(2,1)S(1)} %bitcast.89), channel_id=1, source_target_pairs={{2,0},{4,2},{6,4},{0,6},{3,1},{5,3},{7,5},{1,7},{10,8},{12,10},{14... | collective-permute-start | bytes 2752520 | tf_op jit(solution)/shard_map/ppermute | solution.py:26
  169.2 38.1 %collective-permute-start.12 = (bf16[224,2048]{1,0:T(8,128)(2,1)S(1)}, bf16[224,2048]{1,0:T(8,128)(2,1)}, u32[]{:S(2)}, u32[]{:S(2)}) collective-permute-start(bf16[224,2048]{1,0:T(8,128)(2,1)S(1)} %bitcast.91), channel_id=1, source_target_pairs={{6,0},{0,2},{2,4},{4,6},{7,1},{1,3},{3,5},{5,7},{14,8},{8,10},{10,... | collective-permute-start | bytes 2752520 | tf_op jit(solution)/shard_map/ppermute | solution.py:26
  172.4 40.8 %collective-permute-start.8 = (bf16[224,2048]{1,0:T(8,128)(2,1)S(1)}, bf16[224,2048]{1,0:T(8,128)(2,1)S(1)}, u32[]{:S(2)}, u32[]{:S(2)}) collective-permute-start(bf16[224,2048]{1,0:T(8,128)(2,1)S(1)} %bitcast.92), channel_id=1, source_target_pairs={{2,0},{4,2},{6,4},{0,6},{3,1},{5,3},{7,5},{1,7},{10,8},{12,10},{14... | collective-permute-start | bytes 2752520 | tf_op jit(solution)/shard_map/ppermute | solution.py:26
  172.4 60.6 %collective-permute-start.9 = (bf16[224,2048]{1,0:T(8,128)(2,1)}, bf16[224,2048]{1,0:T(8,128)(2,1)}, u32[]{:S(2)}, u32[]{:S(2)}) collective-permute-start(bf16[224,2048]{1,0:T(8,128)(2,1)} %refs_6_.1), channel_id=1, source_target_pairs={{2,0},{4,2},{6,4},{0,6},{3,1},{5,3},{7,5},{1,7},{10,8},{12,10},{14... | collective-permute-start | bytes 2752520 | tf_op jit(solution)/shard_map/ppermute | solution.py:26
  201.4 32.8 %slice-start = ((bf16[128,1152]{1,0:T(8,128)(2,1)}), bf16[128,128]{1,0:T(8,128)(2,1)S(1)}, s32[]{:S(2)}) async-start(bf16[128,1152]{1,0:T(8,128)(2,1)} %copy-done.12), calls=%async_computation.2 | async-start | bytes 65536 | tf_op jit(solution)/shard_map/slice | solution.py:244
  201.4 70.2 %copy-start.18 = (bf16[2048]{0:T(1024)(128)(2,1)S(1)}, bf16[2048]{0:T(1024)(128)(2,1)}, u32[]{:S(2)}) copy-start(bf16[2048]{0:T(1024)(128)(2,1)} %param.49) | copy-start | bytes 12292
  201.4 31.8 %collective-permute-start.13 = (bf16[224,2048]{1,0:T(8,128)(2,1)S(1)}, bf16[224,2048]{1,0:T(8,128)(2,1)S(1)}, u32[]{:S(2)}, u32[]{:S(2)}) collective-permute-start(bf16[224,2048]{1,0:T(8,128)(2,1)S(1)} %copy-done.5), channel_id=1, source_target_pairs={{6,0},{0,2},{2,4},{4,6},{7,1},{1,3},{3,5},{5,7},{14,8},{8,10},{10,... | collective-permute-start | bytes 2752520 | tf_op jit(solution)/shard_map/ppermute | solution.py:26
  205.1 28.1 %copy-start.3 = (f32[128,2048]{1,0:T(8,128)}, f32[128,2048]{1,0:T(8,128)S(1)}, u32[]{:S(2)}) copy-start(f32[128,2048]{1,0:T(8,128)S(1)} %get-tuple-element.11) | copy-start | bytes 3145732
  205.1 33.2 %collective-permute-start.18 = (bf16[144,2048]{1,0:T(8,128)(2,1)}, bf16[144,2048]{1,0:T(8,128)(2,1)}, u32[]{:S(2)}, u32[]{:S(2)}) collective-permute-start(bf16[144,2048]{1,0:T(8,128)(2,1)} %collective-permute-done.14.refs_15_), channel_id=1, source_target_pairs={{6,0},{0,2},{2,4},{4,6},{7,1},{1,3},{3,5},{5,7},{14,8},{8,10},{10,... | collective-permute-start | bytes 1769480 | tf_op jit(solution)/shard_map/ppermute | solution.py:26
  207.3 45.4 %collective-permute-start.15 = (bf16[224,2048]{1,0:T(8,128)(2,1)}, bf16[224,2048]{1,0:T(8,128)(2,1)}, u32[]{:S(2)}, u32[]{:S(2)}) collective-permute-start(bf16[224,2048]{1,0:T(8,128)(2,1)} %collective-permute-done.7.refs_8_), channel_id=1, source_target_pairs={{2,0},{4,2},{6,4},{0,6},{3,1},{5,3},{7,5},{1,7},{10,8},{12,10},{14... | collective-permute-start | bytes 2752520 | tf_op jit(solution)/shard_map/ppermute | solution.py:26
  213.2 20.0 %copy-start.6 = (bf16[224,2048]{1,0:T(8,128)(2,1)}, bf16[224,2048]{1,0:T(8,128)(2,1)S(1)}, u32[]{:S(2)}) copy-start(bf16[224,2048]{1,0:T(8,128)(2,1)S(1)} %collective-permute-done.8.refs_9_) | copy-start | bytes 2752516
  213.2 39.4 %collective-permute-start.16 = (bf16[224,2048]{1,0:T(8,128)(2,1)}, bf16[224,2048]{1,0:T(8,128)(2,1)}, u32[]{:S(2)}, u32[]{:S(2)}) collective-permute-start(bf16[224,2048]{1,0:T(8,128)(2,1)} %collective-permute-done.12.refs_13_), channel_id=1, source_target_pairs={{6,0},{0,2},{2,4},{4,6},{7,1},{1,3},{3,5},{5,7},{14,8},{8,10},{10,... | collective-permute-start | bytes 2752520 | tf_op jit(solution)/shard_map/ppermute | solution.py:26
  233.0 38.5 %collective-permute-start.17 = (bf16[224,2048]{1,0:T(8,128)(2,1)}, bf16[224,2048]{1,0:T(8,128)(2,1)}, u32[]{:S(2)}, u32[]{:S(2)}) collective-permute-start(bf16[224,2048]{1,0:T(8,128)(2,1)} %collective-permute-done.9.refs_10_), channel_id=1, source_target_pairs={{2,0},{4,2},{6,4},{0,6},{3,1},{5,3},{7,5},{1,7},{10,8},{12,10},{14... | collective-permute-start | bytes 2752520 | tf_op jit(solution)/shard_map/ppermute | solution.py:26
  233.2 0.9 copy-start.7
  234.1 4.2 %collective-permute-start.6 = (bf16[128,2048]{1,0:T(8,128)(2,1)S(1)}, bf16[128,2048]{1,0:T(8,128)(2,1)}, u32[]{:S(2)}, u32[]{:S(2)}) collective-permute-start(bf16[128,2048]{1,0:T(8,128)(2,1)S(1)} %multiply_convert_fusion.refs_0_), channel_id=1, source_target_pairs={{0,1},{1,0},{2,3},{3,2},{4,5},{5,4},{6,7},{7,6},{8,9},{9,8},{10,11... | collective-permute-start | bytes 1572872 | tf_op jit(solution)/shard_map/ppermute | solution.py:294
  284.9 2.0 collective-permute-start.19
  289.1 33.8 %all-to-all-start.1 = ((bf16[16,8,2048]{2,1,0:T(8,128)(2,1)}), bf16[16,8,2048]{2,1,0:T(8,128)(2,1)S(1)}, u32[]{:S(2)}, u32[]{:S(2)}) async-start(bf16[16,8,2048]{2,1,0:T(8,128)(2,1)} %fusion.15), calls=%async_computation.1 | async-start | bytes 1048576 | tf_op jit(solution)/shard_map/all_to_all | solution.py:305

commit v3 on v2

v3 whole, which is shorter than its diff:
```python
import jax
import jax.numpy as jnp
from jax.experimental import pallas as pl
from jax.experimental.pallas import tpu as pltpu
from jax import lax
from jax.sharding import Mesh
from jax.sharding import PartitionSpec as P


LANE_WIDTH = 64
FF_E = 7168
Z = ("ep_0", "ep_1")
X = "ep_2"
EP = ("ep_0", "ep_1", "ep_2")
GRP_EP = ("grp", *EP)
EP_TP = (*EP, "tp")
GRP_EP_TP = ("grp", *EP, "tp")
NEAR = (-1, 0, 1, 2)


RMS_EPS = 1e-06
GROUP_EPS = 0.00064
BF16 = jnp.bfloat16
F32 = jnp.float32


def from_ahead(value, axis, steps):
    size = lax.axis_size(axis)
    return lax.ppermute(value, axis, [((i + steps) % size, i) for i in range(size)])


def turned_lanes(width, x_count, x_rank):
    block = width // x_count
    rows = lax.broadcasted_iota(jnp.int32, (width, width), 0)
    columns = lax.broadcasted_iota(jnp.int32, (width, width), 1)
    moved = rows + x_rank * block
    return (jnp.where(moved >= width, moved - width, moved) == columns).astype(BF16)


def rms_norm(values, norm_gain):
    mean_sq = jnp.mean(values * values, axis=-1, keepdims=True)
    return values * lax.rsqrt(mean_sq + RMS_EPS) * norm_gain


def rows_dot(left, right_rows):
    return lax.dot_general(left, right_rows, (((1,), (1,)), ((), ())), preferred_element_type=F32)


def evolve_kernel(
    memory_ref, query_ref, key_ref, value_ref, decay_ref, rate_ref, scaling_ref, reward_ref,
    after_ref, attended_ref, readout_ref,
):
    rows, heads, width, _ = memory_ref.shape
    eye = (
        lax.broadcasted_iota(jnp.int32, (width, width), 0)
        == lax.broadcasted_iota(jnp.int32, (width, width), 1)
    ).astype(F32).astype(BF16)

    def one_row(r, carry):
        query, key, value = query_ref[r], key_ref[r], value_ref[r]
        decay, rate = decay_ref[r], rate_ref[r]
        unit = key * lax.rsqrt(jnp.sum(key * key, axis=-1, keepdims=True) + 1.0)
        erase = unit * rate
        write = key * rate
        for h in range(heads):
            memory = memory_ref[r, h]
            removal = jnp.sum(memory * unit[h : h + 1], axis=-1, keepdims=True)
            spread_value = jnp.broadcast_to(value[h : h + 1], (width, width)).astype(BF16)
            after = (
                memory * decay[h : h + 1]
                - removal * erase[h : h + 1]
                + rows_dot(eye, spread_value) * write[h : h + 1]
            )
            after_ref[r, h] = after
            high = after.astype(BF16)
            low = (after - high.astype(F32)).astype(BF16)
            wanted = jnp.broadcast_to(query[h : h + 1], (16, width)).astype(BF16)
            readout_ref[h : h + 1] = (rows_dot(wanted, high) + rows_dot(wanted, low))[:1]
        readout = readout_ref[...]
        centred = readout - jnp.mean(readout, axis=-1, keepdims=True)
        variance = jnp.mean(centred * centred, axis=-1, keepdims=True)
        bonus = jnp.sum(query * write * reward_ref[...], axis=-1, keepdims=True)
        attended_ref[r] = (
            centred * lax.rsqrt(variance + GROUP_EPS) * scaling_ref[...] + bonus * value
        ).astype(BF16)
        return carry

    lax.fori_loop(0, rows, one_row, 0)


def evolve_memory(memory, query, key, value, decay, rate, scaling, reward):
    rows, heads, width, _ = memory.shape
    step = rows // 4
    lanes = pl.BlockSpec((step, heads, width), lambda i: (i, 0, 0))
    fixed = pl.BlockSpec((heads, width), lambda i: (0, 0))
    state = pl.BlockSpec((step, heads, width, width), lambda i: (i, 0, 0, 0))
    return pl.pallas_call(
        evolve_kernel,
        grid=(rows // step,),
        in_specs=[state] + [lanes] * 5 + [fixed] * 2,
        out_specs=[state, lanes],
        out_shape=[
            jax.ShapeDtypeStruct(memory.shape, F32),
            jax.ShapeDtypeStruct((rows, heads, width), BF16),
        ],
        scratch_shapes=[pltpu.VMEM((heads, width), F32)],
        name="evolve",
    )(memory, query, key, value, decay, rate, scaling, reward)


def ffn_kernel(pieces, wide, slim, own_ref, other_ref, share_ref, switch_ref, *refs):
    weights, (kept_ref, sent_ref, held, tokens, total, sems) = refs[: 4 * pieces], refs[4 * pieces :]
    block = wide + slim
    copies = []
    for p in range(pieces):
        gate, up, down, common = weights[4 * p : 4 * p + 4]
        parts = []
        for k, ref in enumerate((gate, up, down)):
            parts.append((ref, held.at[p, pl.ds(k * block, wide)]))
            parts.append((common.at[pl.ds(k * slim, slim)], held.at[p, pl.ds(k * block + wide, slim)]))
        copies.append([pltpu.make_async_copy(a, b, sems.at[p, n]) for n, (a, b) in enumerate(parts)])
    for group in copies:
        for copy in group:
            copy.start()
    half = own_ref.shape[0]
    width = tokens.shape[1]
    tokens[:half] = own_ref[:, :width]
    tokens[half:] = other_ref[:, :width]
    every = tokens[...]
    share = share_ref[...]
    branch = jax.nn.sigmoid(rows_dot(switch_ref[...], every)[:1])
    for p in range(pieces):
        for copy in copies[p]:
            copy.wait()
        both = rows_dot(held[p, : 2 * block], every)
        gate_val, up_val = both[:block], both[block:]
        row = lax.broadcasted_iota(jnp.int32, (block, 1), 0)
        scale = jnp.where(row < wide, share, branch)
        hidden = (gate_val * jax.nn.sigmoid(gate_val) * up_val * scale).astype(BF16)
        term = lax.dot_general(
            hidden, held[p, 2 * block :], (((0,), (0,)), ((), ())), preferred_element_type=F32
        )
        if p == 0:
            total[...] = term
        elif p < pieces - 1:
            total[...] += term
        else:
            term = total[...] + term
            kept_ref[...] = term[:half]
            sent_ref[...] = term[half:].astype(BF16)


def ffn(own_in, other_in, share, switch, pieces):
    half, width = own_in.shape[0], switch.shape[1]
    wide, slim = pieces[0][0].shape[0], pieces[0][3].shape[0] // 3
    count = len(pieces)
    vmem = pl.BlockSpec(memory_space=pltpu.VMEM)
    hbm = pl.BlockSpec(memory_space=pl.ANY)
    return pl.pallas_call(
        lambda *refs: ffn_kernel(count, wide, slim, *refs),
        in_specs=[vmem] * 4 + [hbm] * (4 * count),
        out_specs=[vmem, vmem],
        out_shape=[
            jax.ShapeDtypeStruct((half, width), F32),
            jax.ShapeDtypeStruct((half, width), BF16),
        ],
        scratch_shapes=[
            pltpu.VMEM((count, 3 * (wide + slim), width), BF16),
            pltpu.VMEM((2 * half, width), BF16),
            pltpu.VMEM((2 * half, width), F32),
            pltpu.SemaphoreType.DMA((count, 6)),
        ],
        compiler_params=pltpu.CompilerParams(vmem_limit_bytes=48 * 1024 * 1024),
        name="ffn",
    )(own_in, other_in, share, switch, *[ref for piece in pieces for ref in piece])


def body(
    fresh_inputs,
    memory_arrays,
    chosen_specialist,
    chosen_coefficient,
    first_rescale,
    second_rescale,
    receiver_projector,
    address_projector,
    content_projector,
    final_projector,
    forget_narrowing,
    forget_widening,
    forget_bias,
    learning_narrowing,
    learning_widening,
    learning_bias,
    lane_scaling,
    instant_reward,
    specialist_switch,
    specialist_expand,
    specialist_contract,
    common_activator,
    common_expand,
    common_contract,
    common_switch,
):
    own_rows, model_width = fresh_inputs.shape
    tp_count = lax.axis_size("tp")
    tp_rank = lax.axis_index("tp")
    z_count = lax.axis_size(Z)
    x_rank, x_count = lax.axis_index(X), lax.axis_size(X)
    far_count, near_rank = lax.axis_size("ep_0"), lax.axis_index("ep_1")
    half_width = model_width // tp_count
    head_count = half_width // LANE_WIDTH
    half_rows = own_rows // tp_count
    swap = [(0, 1), (1, 0)]

    def pick(value, rank, width, dim):
        return lax.dynamic_slice_in_dim(value, rank * width, width, dim)

    def ring_piece(value, steps):
        return value if steps == 0 else from_ahead(value, Z, steps % z_count)

    def row_piece(value, steps):
        return value if steps == 0 else from_ahead(value, X, steps)

    qkv_rows = jnp.stack(
        (receiver_projector.T, address_projector.T, content_projector.T)
    )
    lane_cols = receiver_projector.shape[1]
    qkv_pieces = [row_piece(qkv_rows, k) for k in range(x_count)]
    expert_cols = specialist_switch.shape[1]
    pad = ((0, -common_activator.shape[1] % 16), (0, 0))
    common = jnp.concatenate(
        [jnp.pad(w, pad) for w in (common_activator.T, common_expand.T, common_contract)]
    )
    own_piece = [specialist_switch.T, specialist_expand.T, specialist_contract, common]
    final_rows = jnp.stack([ring_piece(final_projector.T, k) for k in NEAR])
    final_pieces = [row_piece(final_rows, k) for k in range(x_count)]
    ahead, behind, across = [], [], []
    for w in own_piece:
        ahead.append(from_ahead(w, X, 1))
        behind.append(from_ahead(w, X, x_count - 1))
    for k in range(len(own_piece)):
        if k % 2 == 0:
            across.append(from_ahead(ahead[k], X, 1))
        else:
            across.append(from_ahead(behind[k], X, x_count - 1))
    pieces = [own_piece, ahead, behind, across]

    ring = lax.all_gather(
        pick(fresh_inputs, tp_rank, half_rows, 0), Z, axis=0, tiled=True
    )
    ring_fresh = ring.astype(F32)
    ring_normed = rms_norm(ring_fresh, first_rescale).astype(BF16)
    got = lax.ppermute(pick(ring_normed, 1 - tp_rank, half_width, 1), "tp", swap)
    mine = pick(ring_normed, tp_rank, half_width, 1).reshape(z_count, 1, half_rows, half_width)
    theirs = got.reshape(z_count, 1, half_rows, half_width)
    first = tp_rank == 0
    ring_half = jnp.concatenate(
        (jnp.where(first, mine, theirs), jnp.where(first, theirs, mine)), axis=1
    ).reshape(z_count * own_rows, half_width)

    qkv_row = jnp.concatenate(qkv_pieces, axis=1).reshape(-1, half_width)
    partial = rows_dot(ring_half, qkv_row).astype(BF16)
    partial = lax.all_to_all(
        partial.reshape(z_count, own_rows, -1), Z, 0, 0, tiled=True
    )
    turn = turned_lanes(x_count * lane_cols, x_count, x_rank)
    partial = jnp.transpose(partial.reshape(z_count, own_rows, 3, -1), (2, 1, 0, 3))
    partial = jnp.dot(partial, turn, preferred_element_type=F32).astype(BF16)
    partial = partial.reshape(3, own_rows, model_width)
    got = lax.ppermute(pick(partial, 1 - tp_rank, half_width, 2), "tp", swap)
    projected = (pick(partial, tp_rank, half_width, 2).astype(F32) + got.astype(F32)).astype(BF16)

    def divide_lanes(channels):
        return channels.astype(F32).reshape(own_rows, head_count, LANE_WIDTH)

    normed = rms_norm(fresh_inputs.astype(F32), first_rescale).astype(BF16)
    decay_mid = jnp.tanh(
        jnp.dot(normed, forget_narrowing, preferred_element_type=F32)
    ).astype(BF16)
    decay_pre = forget_bias + jnp.dot(decay_mid, forget_widening, preferred_element_type=F32)
    decay_vals = jnp.exp(-jnp.exp(-jax.nn.softplus(-decay_pre) - 0.5))
    rate_mid = jnp.dot(normed, learning_narrowing, preferred_element_type=F32).astype(BF16)
    rate_vals = jax.nn.sigmoid(
        learning_bias + jnp.dot(rate_mid, learning_widening, preferred_element_type=F32)
    )
    memory_after, attended = evolve_memory(
        memory_arrays,
        divide_lanes(projected[0]),
        divide_lanes(projected[1]),
        divide_lanes(projected[2]),
        divide_lanes(decay_vals),
        divide_lanes(rate_vals),
        lane_scaling.reshape(head_count, LANE_WIDTH),
        instant_reward,
    )

    names = lax.broadcasted_iota(jnp.int32, (own_rows, 128), 1)
    share_table = jnp.zeros((own_rows, 128), F32)
    for k in range(chosen_specialist.shape[1]):
        share_table += jnp.where(
            chosen_specialist[:, k : k + 1] == names, chosen_coefficient[:, k : k + 1].astype(F32), 0.0
        )
    attended = jnp.concatenate(
        (attended.reshape(own_rows, half_width), share_table.astype(BF16)), axis=1
    )
    far = lax.all_gather(attended, "ep_0", axis=0, tiled=True)
    far_share = pick(far[:, half_width:].reshape(far_count, own_rows, -1), tp_rank, half_rows, 1)
    final_row = jnp.concatenate(final_pieces, axis=1).reshape(-1, half_width)
    far_part = rows_dot(far[:, :half_width], final_row).astype(BF16)
    far_part = far_part.reshape(far_count, own_rows, -1)
    got = lax.ppermute(pick(far_part, 1 - tp_rank, half_rows, 1), "tp", swap)
    far_rows = far_count * half_rows
    mixed = (pick(far_part, tp_rank, half_rows, 1).astype(F32) + got.astype(F32)).astype(BF16)
    mixed = mixed.reshape(far_rows, -1)
    mixed = lax.all_gather(mixed[None], "ep_0", axis=0, tiled=True)
    mixed = jnp.swapaxes(mixed.reshape(far_count, far_rows, len(NEAR), -1), 1, 2)
    mixed = mixed.reshape(z_count, far_rows, -1)
    mixed = lax.dynamic_slice_in_dim(
        jnp.concatenate((mixed, mixed)), (z_count - NEAR[0] - near_rank) % z_count, z_count, 0
    )
    mixed = jnp.dot(mixed, turn, preferred_element_type=F32).astype(BF16)
    mixed = jnp.swapaxes(mixed, 0, 1).reshape(far_rows, model_width)
    far_fresh = pick(
        ring_fresh.reshape(far_count, len(NEAR), half_rows, model_width), near_rank, 1, 1
    ).reshape(far_rows, model_width)
    residual = far_fresh + mixed.astype(F32)
    far_in = rms_norm(residual, second_rescale).astype(BF16)
    far_in = jnp.concatenate((far_in, far_share.reshape(far_rows, -1)), axis=1)
    own_in = jnp.concatenate([ring_piece(far_in, k) for k in NEAR])
    other_in = lax.ppermute(own_in, "tp", swap)

    flat_rank = lax.axis_index(EP) * tp_count + tp_rank
    expert = flat_rank * expert_cols // FF_E
    share = jnp.concatenate((own_in[:, model_width:], other_in[:, model_width:])).astype(F32)
    lane = lax.broadcasted_iota(jnp.int32, share.shape, 1)
    expert_share = jnp.sum(jnp.where(lane == expert, share, 0.0), axis=1)[None, :]
    switch = jnp.broadcast_to(common_switch[None, :], (16, model_width))
    kept, sent = ffn(own_in, other_in, expert_share, switch, pieces)
    got = lax.ppermute(sent, "tp", swap)
    near_total = (kept + got.astype(F32)).astype(BF16).reshape(len(NEAR), far_rows, model_width)
    far_total = sum(
        ring_piece(near_total[n], -k).astype(F32) for n, k in enumerate(NEAR)
    ).astype(BF16)
    blocks = lax.all_to_all(
        far_total.reshape(far_count, half_rows, model_width), "ep_0", 0, 0, tiled=True
    )
    routed = jnp.sum(blocks.astype(F32), axis=0)
    own_residual = pick(residual, lax.axis_index("ep_0"), half_rows, 0)
    return ((own_residual + routed).astype(BF16), memory_after)


def solution(mesh):
    torus = Mesh(
        mesh.devices.reshape(mesh.shape["grp"], 4, 4, 4, mesh.shape["tp"]),
        ("grp", *EP, "tp"),
    )
    return jax.shard_map(
        body,
        mesh=torus,
        in_specs=(
            P(GRP_EP, None),
            P(GRP_EP, "tp", None, None),
            P(GRP_EP, None),
            P(GRP_EP, None),
            P(),
            P(),
            P("tp", EP),
            P("tp", EP),
            P("tp", EP),
            P("tp", EP),
            P(),
            P(None, "tp"),
            P("tp"),
            P(),
            P(None, "tp"),
            P("tp"),
            P("tp"),
            P("tp", None),
            P(None, EP_TP),
            P(None, EP_TP),
            P(EP_TP, None),
            P(None, EP_TP),
            P(None, EP_TP),
            P(EP_TP, None),
            P(),
        ),
        out_specs=(P(GRP_EP_TP, None), P(GRP_EP, "tp", None, None)),
        check_vma=False,
    )
```

time: 325 us -> 347 us (1.068)
  the two profiles are of different devices: /device:TPU:38 before, /device:TPU:33 now
where the time goes in v3:
time: 347 us; the launch traced here: 344 us
  waiting for transfers between devices  113 us (33%)
  starting transfers between devices  90.4 us (26%)
  blocking collectives  57.9 us (17%)
  Pallas kernels  43.2 us (12%)
  local copies, waits for them, and re-layouts  16.2 us (5%)
  other arithmetic  16.2 us (5%)
  matrix products  6.01 us (2%)
    ppermute x27, waiting for transfers between devices, from_ahead(): lax.ppermute(value, axis, [((i + steps) % size, i) for i in range(size)])  91.9 us
    ppermute x27, starting transfers between devices, from_ahead(): lax.ppermute(value, axis, [((i + steps) % size, i) for i in range(size)])  52.5 us
    pallas_call x1, Pallas kernels, evolve_memory(): pl.pallas_call(evolve_kernel, grid=(rows // step,), in_specs=[state] + [l...  30.4 us
    all_gather x1, blocking collectives, body(): lax.all_gather(pick(fresh_inputs, tp_rank, half_rows, 0), Z, axis=0, tile...  22.9 us
    all_gather x1, blocking collectives, body(): far = lax.all_gather(attended, 'ep_0', axis=0, tiled=True)  19.7 us
    all_gather x1, blocking collectives, body(): mixed = lax.all_gather(mixed[None], 'ep_0', axis=0, tiled=True)  15.3 us
    all_to_all x1, waiting for transfers between devices, body(): lax.all_to_all(far_total.reshape(far_count, half_rows, model_width), 'ep_...  13.6 us
    pallas_call x1, Pallas kernels, ffn(): pl.pallas_call(lambda *refs: ffn_kernel(count, wide, slim, *refs), in_spe...  12.9 us
  transfers between devices with their start and end apart: 34, of which 18 were waited for; matrix products, arithmetic and copies ran while one was open for 9% of the time, Pallas kernels for 9%

profile of v3, /device:TPU:33, one launch (start us, length us, event | category | flops | bytes accessed | tf_op | source)
XLA Modules:
  0.0 344.1 jit_solution(11009649801313100470)
XLA Ops:
  0.7 1.0 pad_maximum_fusion.5
  1.7 2.3 collective-permute-start.3
  4.0 2.7 collective-permute-start.2
  6.7 1.0 collective-permute-start.1
  7.8 22.1 %collective-permute-start.6 = (bf16[32,1024]{1,0:T(8,128)(2,1)}, bf16[32,1024]{1,0:T(8,128)(2,1)}, u32[]{:S(2)}, u32[]{:S(2)}) collective-permute-start(bf16[32,1024]{1,0:T(8,128)(2,1)} %bitcast.109), channel_id=1, source_target_pairs={{8,0},{16,8},{24,16},{32,24},{40,32},{48,40},{56,48},{64,56},{72,6... | collective-permute-start | bytes 196616 | tf_op jit(solution)/shard_map/ppermute | solution.py:29
  30.6 22.9 %all_gather.9 = bf16[128,2048]{1,0:T(8,128)(2,1)S(1)} all-gather(bf16[8,2048]{1,0:T(8,128)(2,1)S(1)} %constant_dynamic-slice_fusion.3), channel_id=1, replica_groups=mesh['grp'=2,'ep_0'=4,'ep_1'=4,'ep_2'=4,'tp'=2] {'ep_0','ep_1'}, dimensions={0}, use_global_device_ids=true | all-gather | bytes 557056 | tf_op jit(solution)/shard_map/all_gather | solution.py:249
  54.7 8.3 %collective-permute-start = (bf16[128,1024]{1,0:T(8,128)(2,1)}, bf16[128,1024]{1,0:T(8,128)(2,1)}, u32[]{:S(2)}, u32[]{:S(2)}) collective-permute-start(bf16[128,1024]{1,0:T(8,128)(2,1)} %constant_dynamic-slice_fusion.2), channel_id=1, source_target_pairs={{0,1},{1,0},{2,3},{3,2},{4,5},{5,4},{6,7},{7,6},{8,9},{9,8},{10,11... | collective-permute-start | bytes 786440 | tf_op jit(solution)/shard_map/ppermute | solution.py:254
  63.7 1.0 fusion.8
  64.7 2.0 fusion.28
  68.2 2.0 collective-permute-start.5
  71.3 1.2 pad_maximum_fusion.1
  72.5 2.3 collective-permute-start.19
  74.9 1.1 select_bitcast_fusion.1
  76.0 1.1 convolution_convert_fusion.1
  77.2 4.3 %all-to-all-start = ((bf16[16,16,384]{2,1,0:T(8,128)(2,1)}), bf16[16,16,384]{2,1,0:T(8,128)(2,1)S(1)}, u32[]{:S(2)}, u32[]{:S(2)}) async-start(bf16[16,16,384]{2,1,0:T(8,128)(2,1)} %bitcast.14), calls=%async_computation | async-start | bytes 393216 | tf_op jit(solution)/shard_map/all_to_all | solution.py:264
  83.7 1.1 bitcast_convert_fusion.2
  84.8 0.9 pad_maximum_fusion.4
  85.9 1.2 collective-permute-start.9
  87.1 1.5 collective-permute-start.8
  88.6 5.0 %all-to-all-done = bf16[16,16,384]{2,1,0:T(8,128)(2,1)S(1)} async-done(((bf16[16,16,384]{2,1,0:T(8,128)(2,1)}), bf16[16,16,384]{2,1,0:T(8,128)(2,1)S(1)}, u32[]{:S(2)}, u32[]{:S(2)}) %all-to-all-start) | async-done | bytes 196640 | tf_op jit(solution)/shard_map/all_to_all | solution.py:264
  94.9 3.3 collective-permute-done.9
  98.2 4.6 %collective-permute-start.4 = (bf16[3,16,1024]{2,1,0:T(8,128)(2,1)S(1)}, bf16[3,16,1024]{2,1,0:T(8,128)(2,1)S(1)}, u32[]{:S(2)}, u32[]{:S(2)}) collective-permute-start(bf16[3,16,1024]{2,1,0:T(8,128)(2,1)S(1)} %constant_dynamic-slice_fusion.1), channel_id=1, source_target_pairs={{0,1},{1,0},{2,3},{3,2},{4,5},{5,4},{6,7},{7,6},{8,9},{9,8},{10,11... | collective-permute-start | bytes 294920 | tf_op jit(solution)/shard_map/ppermute | solution.py:271
  102.8 1.2 pad_maximum_fusion
  104.7 1.6 reshape.197.value_ref
  107.7 30.4 %evolve.1 = (f32[16,16,64,64]{3,2,1,0:T(8,128)}, bf16[16,16,64]{2,1,0:T(8,128)(2,1)}) custom-call(f32[16,16,64,64]{3,2,1,0:T(8,128)} %memory_ref.1, f32[16,16,64]{2,1,0:T(8,128)} %reshape.195.query_ref, f32[16,16,64]{2,1,0:T(8,128)} %reshape.196.key_ref, f32[16,16,64]{2,1,0:T(8,128)} %reshape.197.value_ref, f32[16,16,64]{2,1,0:T(8,128)} %reshape.185.decay_ref, ...), custom_call_target="tpu_custom_call" | custom-call | tf_op jit(solution)/shard_map/evolve/pallas_call | solution.py:97
  138.1 1.0 reshape.188
  139.1 19.7 %all_gather.10 = bf16[64,1152]{1,0:T(8,128)(2,1)S(1)} all-gather(bf16[16,1152]{1,0:T(8,128)(2,1)S(1)} %pad_maximum_fusion.8), channel_id=1, replica_groups=mesh['grp'=2,'ep_0'=4,'ep_1'=4,'ep_2'=4,'tp'=2] {'ep_0'}, dimensions={0}, use_global_device_ids=true | all-gather | bytes 184320 | tf_op jit(solution)/shard_map/all_gather | solution.py:307
  159.2 3.6 %collective-permute-start.11 = (bf16[4,8,512]{2,1,0:T(8,128)(2,1)S(1)}, bf16[4,8,512]{2,1,0:T(8,128)(2,1)S(1)}, u32[]{:S(2)}, u32[]{:S(2)}) collective-permute-start(bf16[4,8,512]{2,1,0:T(8,128)(2,1)S(1)} %constant_dynamic-slice_fusion), channel_id=1, source_target_pairs={{0,1},{1,0},{2,3},{3,2},{4,5},{5,4},{6,7},{7,6},{8,9},{9,8},{10,11... | collective-permute-start | bytes 98312 | tf_op jit(solution)/shard_map/ppermute | solution.py:312
  163.7 15.3 %all_gather.11 = bf16[4,32,512]{2,1,0:T(8,128)(2,1)S(1)} all-gather(bf16[1,32,512]{2,1,0:T(8,128)(2,1)S(1)} %fusion.33), channel_id=1, replica_groups=mesh['grp'=2,'ep_0'=4,'ep_1'=4,'ep_2'=4,'tp'=2] {'ep_0'}, dimensions={0}, use_global_device_ids=true | all-gather | bytes 163840 | tf_op jit(solution)/shard_map/all_gather | solution.py:316
  179.1 1.1 fusion.4
  181.0 1.7 reshape.201
  182.7 1.1 fusion.14
  184.4 1.3 rsqrt.30
  185.7 1.7 multiply_convert_fusion.1
  188.2 1.2 collective-permute-start.12
  189.3 2.9 collective-permute-start.16
  192.2 1.7 collective-permute-done.14
  193.9 1.9 collective-permute-done.13
  195.9 1.5 collective-permute-start.17
  198.2 6.2 %collective-permute-start.15 = (bf16[128,2176]{1,0:T(8,128)(2,1)S(1)}, bf16[128,2176]{1,0:T(8,128)(2,1)S(1)}, u32[]{:S(2)}, u32[]{:S(2)}) collective-permute-start(bf16[128,2176]{1,0:T(8,128)(2,1)S(1)} %pad_maximum_fusion.2.refs_0_), channel_id=1, source_target_pairs={{0,1},{1,0},{2,3},{3,2},{4,5},{5,4},{6,7},{7,6},{8,9},{9,8},{10,11... | collective-permute-start | bytes 1671176 | tf_op jit(solution)/shard_map/ppermute | solution.py:331
  204.4 3.8 %collective-permute-done.16.refs_8_ = bf16[224,2048]{1,0:T(8,128)(2,1)} collective-permute-done((bf16[224,2048]{1,0:T(8,128)(2,1)S(1)}, bf16[224,2048]{1,0:T(8,128)(2,1)}, u32[]{:S(2)}, u32[]{:S(2)}) %collective-permute-start.16) | collective-permute-done | bytes 917536 | tf_op jit(solution)/shard_map/ppermute | solution.py:29
  208.5 3.7 %collective-permute-done.21.refs_13_ = bf16[224,2048]{1,0:T(8,128)(2,1)} collective-permute-done((bf16[224,2048]{1,0:T(8,128)(2,1)S(1)}, bf16[224,2048]{1,0:T(8,128)(2,1)}, u32[]{:S(2)}, u32[]{:S(2)}) %collective-permute-start.21) | collective-permute-done | bytes 917536 | tf_op jit(solution)/shard_map/ppermute | solution.py:29
  212.1 1.4 collective-permute-start.24
  213.5 14.4 %collective-permute-done.17.refs_9_ = bf16[224,2048]{1,0:T(8,128)(2,1)S(1)} collective-permute-done((bf16[224,2048]{1,0:T(8,128)(2,1)S(1)}, bf16[224,2048]{1,0:T(8,128)(2,1)S(1)}, u32[]{:S(2)}, u32[]{:S(2)}) %collective-permute-start.17) | collective-permute-done | bytes 917536 | tf_op jit(solution)/shard_map/ppermute | solution.py:29
  228.1 19.5 %collective-permute-done.18.refs_10_ = bf16[224,2048]{1,0:T(8,128)(2,1)} collective-permute-done((bf16[224,2048]{1,0:T(8,128)(2,1)}, bf16[224,2048]{1,0:T(8,128)(2,1)}, u32[]{:S(2)}, u32[]{:S(2)}) %collective-permute-start.18) | collective-permute-done | bytes 917536 | tf_op jit(solution)/shard_map/ppermute | solution.py:29
  247.6 3.4 collective-permute-start.26
  252.7 10.3 %collective-permute-done.27.refs_19_ = bf16[144,2048]{1,0:T(8,128)(2,1)} collective-permute-done((bf16[144,2048]{1,0:T(8,128)(2,1)}, bf16[144,2048]{1,0:T(8,128)(2,1)}, u32[]{:S(2)}, u32[]{:S(2)}) %collective-permute-start.27) | collective-permute-done | bytes 589856 | tf_op jit(solution)/shard_map/ppermute | solution.py:29
  263.1 4.2 %collective-permute-done.24.refs_16_ = bf16[224,2048]{1,0:T(8,128)(2,1)} collective-permute-done((bf16[224,2048]{1,0:T(8,128)(2,1)}, bf16[224,2048]{1,0:T(8,128)(2,1)}, u32[]{:S(2)}, u32[]{:S(2)}) %collective-permute-start.24) | collective-permute-done | bytes 917536 | tf_op jit(solution)/shard_map/ppermute | solution.py:29
  267.3 19.7 %collective-permute-done.26.refs_18_ = bf16[224,2048]{1,0:T(8,128)(2,1)} collective-permute-done((bf16[224,2048]{1,0:T(8,128)(2,1)}, bf16[224,2048]{1,0:T(8,128)(2,1)}, u32[]{:S(2)}, u32[]{:S(2)}) %collective-permute-start.26) | collective-permute-done | bytes 917536 | tf_op jit(solution)/shard_map/ppermute | solution.py:29
  287.0 1.0 copy-done.4
  288.0 1.1 copy-done.6
  289.1 12.9 %ffn.1 = (f32[128,2048]{1,0:T(8,128)}, bf16[128,2048]{1,0:T(8,128)(2,1)S(1)}) custom-call(bf16[128,2176]{1,0:T(8,128)(2,1)S(1)} %pad_maximum_fusion.2.refs_0_, bf16[128,2176]{1,0:T(8,128)(2,1)S(1)} %copy-done.4, f32[1,256]{1,0:T(1,128)S(1)} %bitcast.96, bf16[16,2048]{1,0:T(8,128)(2,1)S(1)} %broadcast_in_dim.58.refs_3_, bf16[224,2048]{1,0:T(8,128)(2,1)S(1)} %bitcast.92, ...), custom_call_target="tpu_custom_call" | custom-call | tf_op jit(solution)/shard_map/ffn/pallas_call | solution.py:159
  302.0 4.7 %collective-permute-start.28 = (bf16[128,2048]{1,0:T(8,128)(2,1)S(1)}, bf16[128,2048]{1,0:T(8,128)(2,1)S(1)}, u32[]{:S(2)}, u32[]{:S(2)}) collective-permute-start(bf16[128,2048]{1,0:T(8,128)(2,1)S(1)} %get-tuple-element.8), channel_id=1, source_target_pairs={{0,1},{1,0},{2,3},{3,2},{4,5},{5,4},{6,7},{7,6},{8,9},{9,8},{10,11... | collective-permute-start | bytes 1572872 | tf_op jit(solution)/shard_map/ppermute | solution.py:340
  306.6 1.5 collective-permute-done.28
  308.2 1.3 add_convert_fusion
  309.6 1.5 collective-permute-start.29
  311.0 1.0 collective-permute-start.31
  312.0 1.3 collective-permute-start.30
  313.4 1.0 collective-permute-done.29
  314.4 5.5 %collective-permute-done.31 = bf16[32,2048]{1,0:T(8,128)(2,1)S(1)} collective-permute-done((bf16[32,2048]{1,0:T(8,128)(2,1)S(1)}, bf16[32,2048]{1,0:T(8,128)(2,1)S(1)}, u32[]{:S(2)}, u32[]{:S(2)}) %collective-permute-start.31) | collective-permute-done | bytes 131104 | tf_op jit(solution)/shard_map/ppermute | solution.py:29
  319.8 2.3 collective-permute-done.30
  322.8 6.3 %all-to-all-start.1 = ((bf16[4,8,2048]{2,1,0:T(8,128)(2,1)}), bf16[4,8,2048]{2,1,0:T(8,128)(2,1)S(1)}, u32[]{:S(2)}, u32[]{:S(2)}) async-start(bf16[4,8,2048]{2,1,0:T(8,128)(2,1)} %fusion.20), calls=%async_computation.1 | async-start | bytes 262144 | tf_op jit(solution)/shard_map/all_to_all | solution.py:345
  329.1 13.6 %all-to-all-done.1 = bf16[4,8,2048]{2,1,0:T(8,128)(2,1)S(1)} async-done(((bf16[4,8,2048]{2,1,0:T(8,128)(2,1)}), bf16[4,8,2048]{2,1,0:T(8,128)(2,1)S(1)}, u32[]{:S(2)}, u32[]{:S(2)}) %all-to-all-start.1) | async-done | bytes 131104 | tf_op jit(solution)/shard_map/all_to_all | solution.py:345
  342.6 1.5 add_convert_fusion.3
  (144 shorter events, 18.3 us)
Async XLA Ops:
  0.6 63.1 %copy-start = (bf16[2048,64]{0,1:T(8,128)(2,1)S(1)}, bf16[2048,64]{0,1:T(8,128)(2,1)}, u32[]{:S(2)}) copy-start(bf16[2048,64]{0,1:T(8,128)(2,1)} %param.38) | copy-start | bytes 786436
  0.6 53.1 %copy-start.23 = (f32[2048]{0:T(1024)S(1)}, f32[2048]{0:T(1024)}, u32[]{:S(2)}) copy-start(f32[2048]{0:T(1024)} %param.29) | copy-start | bytes 24580
  0.7 62.4 %copy-start.20 = (bf16[16,2048]{1,0:T(8,128)(2,1)S(1)}, bf16[16,2048]{1,0:T(8,128)(2,1)}, u32[]{:S(2)}) copy-start(bf16[16,2048]{1,0:T(8,128)(2,1)} %param.25) | copy-start | bytes 196612
  0.7 62.5 %copy-start.28 = (s32[16,2]{0,1:T(2,128)S(1)}, s32[16,2]{0,1:T(2,128)}, u32[]{:S(2)}) copy-start(s32[16,2]{0,1:T(2,128)} %param.27) | copy-start | bytes 388
  0.7 62.5 %copy-start.27 = (bf16[16,2]{0,1:T(2,128)(2,1)S(1)}, bf16[16,2]{0,1:T(2,128)(2,1)}, u32[]{:S(2)}) copy-start(bf16[16,2]{0,1:T(2,128)(2,1)} %param.28) | copy-start | bytes 196
  0.7 63.0 %copy-start.33 = (bf16[64,1024]{1,0:T(8,128)(2,1)S(1)}, bf16[64,1024]{1,0:T(8,128)(2,1)}, u32[]{:S(2)}) copy-start(bf16[64,1024]{1,0:T(8,128)(2,1)} %param.39) | copy-start | bytes 393220
  0.7 63.0 %copy-start.34 = (f32[1024]{0:T(1024)S(1)}, f32[1024]{0:T(1024)}, u32[]{:S(2)}) copy-start(f32[1024]{0:T(1024)} %param.40) | copy-start | bytes 12292
  1.7 65.8 %collective-permute-start.3 = (bf16[3,32,1024]{2,1,0:T(8,128)(2,1)S(1)}, bf16[3,32,1024]{2,1,0:T(8,128)(2,1)S(1)}, u32[]{:S(2)}, u32[]{:S(2)}) collective-permute-start(bf16[3,32,1024]{2,1,0:T(8,128)(2,1)S(1)} %pad_maximum_fusion.5), channel_id=1, source_target_pairs={{6,0},{0,2},{2,4},{4,6},{7,1},{1,3},{3,5},{5,7},{14,8},{8,10},{10,... | collective-permute-start | bytes 589832 | tf_op jit(solution)/shard_map/ppermute | solution.py:29
  4.0 64.2 %collective-permute-start.2 = (bf16[3,32,1024]{2,1,0:T(8,128)(2,1)S(1)}, bf16[3,32,1024]{2,1,0:T(8,128)(2,1)S(1)}, u32[]{:S(2)}, u32[]{:S(2)}) collective-permute-start(bf16[3,32,1024]{2,1,0:T(8,128)(2,1)S(1)} %pad_maximum_fusion.5), channel_id=1, source_target_pairs={{4,0},{6,2},{0,4},{2,6},{5,1},{7,3},{1,5},{3,7},{12,8},{14,10},{8,... | collective-permute-start | bytes 589832 | tf_op jit(solution)/shard_map/ppermute | solution.py:29
  6.7 63.5 %collective-permute-start.1 = (bf16[3,32,1024]{2,1,0:T(8,128)(2,1)S(1)}, bf16[3,32,1024]{2,1,0:T(8,128)(2,1)S(1)}, u32[]{:S(2)}, u32[]{:S(2)}) collective-permute-start(bf16[3,32,1024]{2,1,0:T(8,128)(2,1)S(1)} %pad_maximum_fusion.5), channel_id=1, source_target_pairs={{2,0},{4,2},{6,4},{0,6},{3,1},{5,3},{7,5},{1,7},{10,8},{12,10},{14... | collective-permute-start | bytes 589832 | tf_op jit(solution)/shard_map/ppermute | solution.py:29
  7.8 77.1 %collective-permute-start.6 = (bf16[32,1024]{1,0:T(8,128)(2,1)}, bf16[32,1024]{1,0:T(8,128)(2,1)}, u32[]{:S(2)}, u32[]{:S(2)}) collective-permute-start(bf16[32,1024]{1,0:T(8,128)(2,1)} %bitcast.109), channel_id=1, source_target_pairs={{8,0},{16,8},{24,16},{32,24},{40,32},{48,40},{56,48},{64,56},{72,6... | collective-permute-start | bytes 196616 | tf_op jit(solution)/shard_map/ppermute | solution.py:29
  30.6 34.1 %copy-start.32 = (bf16[2048,64]{0,1:T(8,128)(2,1)S(1)}, bf16[2048,64]{0,1:T(8,128)(2,1)}, u32[]{:S(2)}) copy-start(bf16[2048,64]{0,1:T(8,128)(2,1)} %param.35) | copy-start | bytes 786436
  30.6 34.1 %copy-start.35 = (f32[1024]{0:T(1024)S(1)}, f32[1024]{0:T(1024)}, u32[]{:S(2)}) copy-start(f32[1024]{0:T(1024)} %param.37) | copy-start | bytes 12292
  53.7 13.1 %copy-start.14 = (bf16[44,2048]{1,0:T(8,128)(2,1)S(1)}, bf16[44,2048]{1,0:T(8,128)(2,1)}, u32[]{:S(2)}) copy-start(bf16[44,2048]{1,0:T(8,128)(2,1)} %param.48) | copy-start | bytes 540676
  53.7 13.1 %copy-start.15 = (bf16[2048,44]{0,1:T(8,128)(2,1)S(1)}, bf16[2048,44]{0,1:T(8,128)(2,1)}, u32[]{:S(2)}) copy-start(bf16[2048,44]{0,1:T(8,128)(2,1)} %param.47) | copy-start | bytes 540676
  53.7 13.0 %copy-start.16 = (bf16[2048,44]{0,1:T(8,128)(2,1)S(1)}, bf16[2048,44]{0,1:T(8,128)(2,1)}, u32[]{:S(2)}) copy-start(bf16[2048,44]{0,1:T(8,128)(2,1)} %param.46) | copy-start | bytes 540676
  53.9 13.6 %copy-start.13 = (bf16[1024,32]{0,1:T(8,128)(2,1)S(1)}, bf16[1024,32]{0,1:T(8,128)(2,1)}, u32[]{:S(2)}) copy-start(bf16[1024,32]{0,1:T(8,128)(2,1)} %param.34) | copy-start | bytes 196612
  53.9 17.4 %copy-start.10 = (bf16[1024,32]{0,1:T(8,128)(2,1)S(1)}, bf16[1024,32]{0,1:T(8,128)(2,1)}, u32[]{:S(2)}) copy-start(bf16[1024,32]{0,1:T(8,128)(2,1)} %param.33) | copy-start | bytes 196612
  53.9 17.4 %copy-start.11 = (bf16[1024,32]{0,1:T(8,128)(2,1)S(1)}, bf16[1024,32]{0,1:T(8,128)(2,1)}, u32[]{:S(2)}) copy-start(bf16[1024,32]{0,1:T(8,128)(2,1)} %param.32) | copy-start | bytes 196612
  54.0 17.4 %copy-start.12 = (bf16[1024,32]{0,1:T(8,128)(2,1)S(1)}, bf16[1024,32]{0,1:T(8,128)(2,1)}, u32[]{:S(2)}) copy-start(bf16[1024,32]{0,1:T(8,128)(2,1)} %param.31) | copy-start | bytes 196612
  54.7 17.8 %collective-permute-start = (bf16[128,1024]{1,0:T(8,128)(2,1)}, bf16[128,1024]{1,0:T(8,128)(2,1)}, u32[]{:S(2)}, u32[]{:S(2)}) collective-permute-start(bf16[128,1024]{1,0:T(8,128)(2,1)} %constant_dynamic-slice_fusion.2), channel_id=1, source_target_pairs={{0,1},{1,0},{2,3},{3,2},{4,5},{5,4},{6,7},{7,6},{8,9},{9,8},{10,11... | collective-permute-start | bytes 786440 | tf_op jit(solution)/shard_map/ppermute | solution.py:254
  67.6 2.7 copy-start.17
  67.6 17.3 %collective-permute-start.7 = (bf16[32,1024]{1,0:T(8,128)(2,1)S(1)}, bf16[32,1024]{1,0:T(8,128)(2,1)}, u32[]{:S(2)}, u32[]{:S(2)}) collective-permute-start(bf16[32,1024]{1,0:T(8,128)(2,1)S(1)} %bitcast.110), channel_id=1, source_target_pairs={{16,0},{24,8},{32,16},{40,24},{48,32},{56,40},{64,48},{72,56},{80,... | collective-permute-start | bytes 196616 | tf_op jit(solution)/shard_map/ppermute | solution.py:29
  68.2 16.7 %collective-permute-start.5 = (bf16[32,1024]{1,0:T(8,128)(2,1)S(1)}, bf16[32,1024]{1,0:T(8,128)(2,1)}, u32[]{:S(2)}, u32[]{:S(2)}) collective-permute-start(bf16[32,1024]{1,0:T(8,128)(2,1)S(1)} %bitcast.111), channel_id=1, source_target_pairs={{120,0},{0,8},{8,16},{16,24},{24,32},{32,40},{40,48},{48,56},{56,6... | collective-permute-start | bytes 196616 | tf_op jit(solution)/shard_map/ppermute | solution.py:29
  70.9 117.3 %collective-permute-start.23 = (bf16[144,2048]{1,0:T(8,128)(2,1)S(1)}, bf16[144,2048]{1,0:T(8,128)(2,1)S(1)}, u32[]{:S(2)}, u32[]{:S(2)}) collective-permute-start(bf16[144,2048]{1,0:T(8,128)(2,1)S(1)} %fusion.12.refs_7_), channel_id=1, source_target_pairs={{6,0},{0,2},{2,4},{4,6},{7,1},{1,3},{3,5},{5,7},{14,8},{8,10},{10,... | collective-permute-start | bytes 1769480 | tf_op jit(solution)/shard_map/ppermute | solution.py:29
  72.5 116.8 %collective-permute-start.19 = (bf16[144,2048]{1,0:T(8,128)(2,1)S(1)}, bf16[144,2048]{1,0:T(8,128)(2,1)}, u32[]{:S(2)}, u32[]{:S(2)}) collective-permute-start(bf16[144,2048]{1,0:T(8,128)(2,1)S(1)} %fusion.12.refs_7_), channel_id=1, source_target_pairs={{2,0},{4,2},{6,4},{0,6},{3,1},{5,3},{7,5},{1,7},{10,8},{12,10},{14... | collective-permute-start | bytes 1769480 | tf_op jit(solution)/shard_map/ppermute | solution.py:29
  75.9 5.6 %copy-start.25 = (f32[1024]{0:T(1024)S(1)}, f32[1024]{0:T(1024)}, u32[]{:S(2)}) copy-start(f32[1024]{0:T(1024)} %param.41) | copy-start | bytes 12292
  76.0 6.3 %copy-start.22 = (f32[16,1024]{1,0:T(8,128)S(1)}, f32[16,1024]{1,0:T(8,128)}, u32[]{:S(2)}) copy-start(f32[16,1024]{1,0:T(8,128)} %fusion.28) | copy-start | bytes 196612
  76.0 7.0 %copy-start.21 = (f32[16,1024]{1,0:T(8,128)S(1)}, f32[16,1024]{1,0:T(8,128)}, u32[]{:S(2)}) copy-start(f32[16,1024]{1,0:T(8,128)} %fusion.8) | copy-start | bytes 196612
  77.2 16.4 %all-to-all-start = ((bf16[16,16,384]{2,1,0:T(8,128)(2,1)}), bf16[16,16,384]{2,1,0:T(8,128)(2,1)S(1)}, u32[]{:S(2)}, u32[]{:S(2)}) async-start(bf16[16,16,384]{2,1,0:T(8,128)(2,1)} %bitcast.14), calls=%async_computation | async-start | bytes 393216 | tf_op jit(solution)/shard_map/all_to_all | solution.py:264
  81.5 12.5 %copy-start.29 = (s32[128]{0:T(128)}, s32[128]{0:T(128)S(1)}, u32[]{:S(2)}) copy-start(s32[128]{0:T(128)S(1)} %get-tuple-element.28) | copy-start | bytes 1540
  81.5 12.5 %copy-start.30 = (s32[128]{0:T(128)}, s32[128]{0:T(128)S(1)}, u32[]{:S(2)}) copy-start(s32[128]{0:T(128)S(1)} %get-tuple-element.29) | copy-start | bytes 1540
  83.7 11.1 %copy-start.1 = (bf16[2048,224]{0,1:T(8,128)(2,1)S(1)}, bf16[2048,224]{0,1:T(8,128)(2,1)}, u32[]{:S(2)}) copy-start(bf16[2048,224]{0,1:T(8,128)(2,1)} %param.43) | copy-start | bytes 2752516
  84.8 17.9 %copy-start.31 = (pred[128]{0:T(512)(128)(4,1)}, pred[128]{0:T(512)(128)(4,1)S(1)}, u32[]{:S(2)}) copy-start(pred[128]{0:T(512)(128)(4,1)S(1)} %broadcast_compare_fusion) | copy-start | bytes 388
  85.8 9.1 %collective-permute-start.10 = (bf16[4,32,1024]{2,1,0:T(8,128)(2,1)S(1)}, bf16[4,32,1024]{2,1,0:T(8,128)(2,1)}, u32[]{:S(2)}, u32[]{:S(2)}) collective-permute-start(bf16[4,32,1024]{2,1,0:T(8,128)(2,1)S(1)} %pad_maximum_fusion.4), channel_id=1, source_target_pairs={{6,0},{0,2},{2,4},{4,6},{7,1},{1,3},{3,5},{5,7},{14,8},{8,10},{10,... | collective-permute-start | bytes 786440 | tf_op jit(solution)/shard_map/ppermute | solution.py:29
  85.9 12.2 %collective-permute-start.9 = (bf16[4,32,1024]{2,1,0:T(8,128)(2,1)S(1)}, bf16[4,32,1024]{2,1,0:T(8,128)(2,1)}, u32[]{:S(2)}, u32[]{:S(2)}) collective-permute-start(bf16[4,32,1024]{2,1,0:T(8,128)(2,1)S(1)} %pad_maximum_fusion.4), channel_id=1, source_target_pairs={{4,0},{6,2},{0,4},{2,6},{5,1},{7,3},{1,5},{3,7},{12,8},{14,10},{8,... | collective-permute-start | bytes 786440 | tf_op jit(solution)/shard_map/ppermute | solution.py:29
  87.1 15.6 %collective-permute-start.8 = (bf16[4,32,1024]{2,1,0:T(8,128)(2,1)S(1)}, bf16[4,32,1024]{2,1,0:T(8,128)(2,1)}, u32[]{:S(2)}, u32[]{:S(2)}) collective-permute-start(bf16[4,32,1024]{2,1,0:T(8,128)(2,1)S(1)} %pad_maximum_fusion.4), channel_id=1, source_target_pairs={{2,0},{4,2},{6,4},{0,6},{3,1},{5,3},{7,5},{1,7},{10,8},{12,10},{14... | collective-permute-start | bytes 786440 | tf_op jit(solution)/shard_map/ppermute | solution.py:29
  94.1 8.6 %copy-start.8 = (bf16[3,16,2048]{2,1,0:T(8,128)(2,1)}, bf16[3,16,2048]{2,1,0:T(8,128)(2,1)S(1)}, u32[]{:S(2)}) copy-start(bf16[3,16,2048]{2,1,0:T(8,128)(2,1)S(1)} %reshape.184) | copy-start | bytes 589828
  94.9 103.4 %collective-permute-start.20 = (bf16[224,2048]{1,0:T(8,128)(2,1)S(1)}, bf16[224,2048]{1,0:T(8,128)(2,1)}, u32[]{:S(2)}, u32[]{:S(2)}) collective-permute-start(bf16[224,2048]{1,0:T(8,128)(2,1)S(1)} %bitcast.90), channel_id=1, source_target_pairs={{6,0},{0,2},{2,4},{4,6},{7,1},{1,3},{3,5},{5,7},{14,8},{8,10},{10,... | collective-permute-start | bytes 2752520 | tf_op jit(solution)/shard_map/ppermute | solution.py:29
  98.2 5.9 %collective-permute-start.4 = (bf16[3,16,1024]{2,1,0:T(8,128)(2,1)S(1)}, bf16[3,16,1024]{2,1,0:T(8,128)(2,1)S(1)}, u32[]{:S(2)}, u32[]{:S(2)}) collective-permute-start(bf16[3,16,1024]{2,1,0:T(8,128)(2,1)S(1)} %constant_dynamic-slice_fusion.1), channel_id=1, source_target_pairs={{0,1},{1,0},{2,3},{3,2},{4,5},{5,4},{6,7},{7,6},{8,9},{9,8},{10,11... | collective-permute-start | bytes 294920 | tf_op jit(solution)/shard_map/ppermute | solution.py:271
  159.2 26.5 %copy-start.24 = (f32[2048]{0:T(1024)S(1)}, f32[2048]{0:T(1024)}, u32[]{:S(2)}) copy-start(f32[2048]{0:T(1024)} %param.30) | copy-start | bytes 24580
  159.2 4.4 %collective-permute-start.11 = (bf16[4,8,512]{2,1,0:T(8,128)(2,1)S(1)}, bf16[4,8,512]{2,1,0:T(8,128)(2,1)S(1)}, u32[]{:S(2)}, u32[]{:S(2)}) collective-permute-start(bf16[4,8,512]{2,1,0:T(8,128)(2,1)S(1)} %constant_dynamic-slice_fusion), channel_id=1, source_target_pairs={{0,1},{1,0},{2,3},{3,2},{4,5},{5,4},{6,7},{7,6},{8,9},{9,8},{10,11... | collective-permute-start | bytes 98312 | tf_op jit(solution)/shard_map/ppermute | solution.py:312
  179.0 14.9 %copy-start.2 = (bf16[2048,224]{0,1:T(8,128)(2,1)S(1)}, bf16[2048,224]{0,1:T(8,128)(2,1)}, u32[]{:S(2)}) copy-start(bf16[2048,224]{0,1:T(8,128)(2,1)} %param.44) | copy-start | bytes 2752516
  187.4 99.6 %copy-start.26 = (bf16[2048]{0:T(1024)(128)(2,1)S(1)}, bf16[2048]{0:T(1024)(128)(2,1)}, u32[]{:S(2)}) copy-start(bf16[2048]{0:T(1024)(128)(2,1)} %param.49) | copy-start | bytes 12292
  187.4 6.5 %collective-permute-start.14 = (bf16[32,2176]{1,0:T(8,128)(2,1)S(1)}, bf16[32,2176]{1,0:T(8,128)(2,1)S(1)}, u32[]{:S(2)}, u32[]{:S(2)}) collective-permute-start(bf16[32,2176]{1,0:T(8,128)(2,1)S(1)} %pad_maximum_fusion.6), channel_id=1, source_target_pairs={{16,0},{24,8},{32,16},{40,24},{48,32},{56,40},{64,48},{72,56},{80,... | collective-permute-start | bytes 417800 | tf_op jit(solution)/shard_map/ppermute | solution.py:29
  187.7 8.2 %collective-permute-start.13 = (bf16[32,2176]{1,0:T(8,128)(2,1)S(1)}, bf16[32,2176]{1,0:T(8,128)(2,1)S(1)}, u32[]{:S(2)}, u32[]{:S(2)}) collective-permute-start(bf16[32,2176]{1,0:T(8,128)(2,1)S(1)} %pad_maximum_fusion.6), channel_id=1, source_target_pairs={{8,0},{16,8},{24,16},{32,24},{40,32},{48,40},{56,48},{64,56},{72,6... | collective-permute-start | bytes 417800 | tf_op jit(solution)/shard_map/ppermute | solution.py:29
  188.2 9.3 %copy-start.5 = (bf16[144,2048]{1,0:T(8,128)(2,1)}, bf16[144,2048]{1,0:T(8,128)(2,1)S(1)}, u32[]{:S(2)}) copy-start(bf16[144,2048]{1,0:T(8,128)(2,1)S(1)} %collective-permute-done.23.refs_15_) | copy-start | bytes 1769476
  188.2 9.3 %collective-permute-start.12 = (bf16[32,2176]{1,0:T(8,128)(2,1)S(1)}, bf16[32,2176]{1,0:T(8,128)(2,1)S(1)}, u32[]{:S(2)}, u32[]{:S(2)}) collective-permute-start(bf16[32,2176]{1,0:T(8,128)(2,1)S(1)} %pad_maximum_fusion.6), channel_id=1, source_target_pairs={{120,0},{0,8},{8,16},{16,24},{24,32},{32,40},{40,48},{48,56},{56,6... | collective-permute-start | bytes 417800 | tf_op jit(solution)/shard_map/ppermute | solution.py:29
  189.3 18.9 %collective-permute-start.16 = (bf16[224,2048]{1,0:T(8,128)(2,1)S(1)}, bf16[224,2048]{1,0:T(8,128)(2,1)}, u32[]{:S(2)}, u32[]{:S(2)}) collective-permute-start(bf16[224,2048]{1,0:T(8,128)(2,1)S(1)} %bitcast.91), channel_id=1, source_target_pairs={{2,0},{4,2},{6,4},{0,6},{3,1},{5,3},{7,5},{1,7},{10,8},{12,10},{14... | collective-permute-start | bytes 2752520 | tf_op jit(solution)/shard_map/ppermute | solution.py:29
  193.9 18.2 %collective-permute-start.21 = (bf16[224,2048]{1,0:T(8,128)(2,1)S(1)}, bf16[224,2048]{1,0:T(8,128)(2,1)}, u32[]{:S(2)}, u32[]{:S(2)}) collective-permute-start(bf16[224,2048]{1,0:T(8,128)(2,1)S(1)} %bitcast.93), channel_id=1, source_target_pairs={{6,0},{0,2},{2,4},{4,6},{7,1},{1,3},{3,5},{5,7},{14,8},{8,10},{10,... | collective-permute-start | bytes 2752520 | tf_op jit(solution)/shard_map/ppermute | solution.py:29
  195.9 32.0 %collective-permute-start.17 = (bf16[224,2048]{1,0:T(8,128)(2,1)S(1)}, bf16[224,2048]{1,0:T(8,128)(2,1)S(1)}, u32[]{:S(2)}, u32[]{:S(2)}) collective-permute-start(bf16[224,2048]{1,0:T(8,128)(2,1)S(1)} %bitcast.94), channel_id=1, source_target_pairs={{2,0},{4,2},{6,4},{0,6},{3,1},{5,3},{7,5},{1,7},{10,8},{12,10},{14... | collective-permute-start | bytes 2752520 | tf_op jit(solution)/shard_map/ppermute | solution.py:29
  197.4 50.2 %collective-permute-start.18 = (bf16[224,2048]{1,0:T(8,128)(2,1)}, bf16[224,2048]{1,0:T(8,128)(2,1)}, u32[]{:S(2)}, u32[]{:S(2)}) collective-permute-start(bf16[224,2048]{1,0:T(8,128)(2,1)} %refs_6_.1), channel_id=1, source_target_pairs={{2,0},{4,2},{6,4},{0,6},{3,1},{5,3},{7,5},{1,7},{10,8},{12,10},{14... | collective-permute-start | bytes 2752520 | tf_op jit(solution)/shard_map/ppermute | solution.py:29
  198.2 52.8 %collective-permute-start.15 = (bf16[128,2176]{1,0:T(8,128)(2,1)S(1)}, bf16[128,2176]{1,0:T(8,128)(2,1)S(1)}, u32[]{:S(2)}, u32[]{:S(2)}) collective-permute-start(bf16[128,2176]{1,0:T(8,128)(2,1)S(1)} %pad_maximum_fusion.2.refs_0_), channel_id=1, source_target_pairs={{0,1},{1,0},{2,3},{3,2},{4,5},{5,4},{6,7},{7,6},{8,9},{9,8},{10,11... | collective-permute-start | bytes 1671176 | tf_op jit(solution)/shard_map/ppermute | solution.py:331
  208.2 44.5 %collective-permute-start.22 = (bf16[224,2048]{1,0:T(8,128)(2,1)}, bf16[224,2048]{1,0:T(8,128)(2,1)}, u32[]{:S(2)}, u32[]{:S(2)}) collective-permute-start(bf16[224,2048]{1,0:T(8,128)(2,1)} %refs_6_.1), channel_id=1, source_target_pairs={{6,0},{0,2},{2,4},{4,6},{7,1},{1,3},{3,5},{5,7},{14,8},{8,10},{10,... | collective-permute-start | bytes 2752520 | tf_op jit(solution)/shard_map/ppermute | solution.py:29
  212.1 55.2 %collective-permute-start.24 = (bf16[224,2048]{1,0:T(8,128)(2,1)}, bf16[224,2048]{1,0:T(8,128)(2,1)}, u32[]{:S(2)}, u32[]{:S(2)}) collective-permute-start(bf16[224,2048]{1,0:T(8,128)(2,1)} %collective-permute-done.16.refs_8_), channel_id=1, source_target_pairs={{2,0},{4,2},{6,4},{0,6},{3,1},{5,3},{7,5},{1,7},{10,8},{12,10},{14... | collective-permute-start | bytes 2752520 | tf_op jit(solution)/shard_map/ppermute | solution.py:29
  227.9 23.2 %copy-start.7 = (bf16[224,2048]{1,0:T(8,128)(2,1)}, bf16[224,2048]{1,0:T(8,128)(2,1)S(1)}, u32[]{:S(2)}) copy-start(bf16[224,2048]{1,0:T(8,128)(2,1)S(1)} %collective-permute-done.17.refs_9_) | copy-start | bytes 2752516
  227.9 39.4 %collective-permute-start.25 = (bf16[224,2048]{1,0:T(8,128)(2,1)}, bf16[224,2048]{1,0:T(8,128)(2,1)}, u32[]{:S(2)}, u32[]{:S(2)}) collective-permute-start(bf16[224,2048]{1,0:T(8,128)(2,1)} %collective-permute-done.21.refs_13_), channel_id=1, source_target_pairs={{6,0},{0,2},{2,4},{4,6},{7,1},{1,3},{3,5},{5,7},{14,8},{8,10},{10,... | collective-permute-start | bytes 2752520 | tf_op jit(solution)/shard_map/ppermute | solution.py:29
  247.6 39.3 %collective-permute-start.26 = (bf16[224,2048]{1,0:T(8,128)(2,1)}, bf16[224,2048]{1,0:T(8,128)(2,1)}, u32[]{:S(2)}, u32[]{:S(2)}) collective-permute-start(bf16[224,2048]{1,0:T(8,128)(2,1)} %collective-permute-done.18.refs_10_), channel_id=1, source_target_pairs={{2,0},{4,2},{6,4},{0,6},{3,1},{5,3},{7,5},{1,7},{10,8},{12,10},{14... | collective-permute-start | bytes 2752520 | tf_op jit(solution)/shard_map/ppermute | solution.py:29
  251.8 11.2 %collective-permute-start.27 = (bf16[144,2048]{1,0:T(8,128)(2,1)}, bf16[144,2048]{1,0:T(8,128)(2,1)}, u32[]{:S(2)}, u32[]{:S(2)}) collective-permute-start(bf16[144,2048]{1,0:T(8,128)(2,1)} %copy-done.5), channel_id=1, source_target_pairs={{6,0},{0,2},{2,4},{4,6},{7,1},{1,3},{3,5},{5,7},{14,8},{8,10},{10,... | collective-permute-start | bytes 1769480 | tf_op jit(solution)/shard_map/ppermute | solution.py:29
  302.0 6.2 %collective-permute-start.28 = (bf16[128,2048]{1,0:T(8,128)(2,1)S(1)}, bf16[128,2048]{1,0:T(8,128)(2,1)S(1)}, u32[]{:S(2)}, u32[]{:S(2)}) collective-permute-start(bf16[128,2048]{1,0:T(8,128)(2,1)S(1)} %get-tuple-element.8), channel_id=1, source_target_pairs={{0,1},{1,0},{2,3},{3,2},{4,5},{5,4},{6,7},{7,6},{8,9},{9,8},{10,11... | collective-permute-start | bytes 1572872 | tf_op jit(solution)/shard_map/ppermute | solution.py:340
  309.6 4.8 %collective-permute-start.29 = (bf16[32,2048]{1,0:T(8,128)(2,1)S(1)}, bf16[32,2048]{1,0:T(8,128)(2,1)S(1)}, u32[]{:S(2)}, u32[]{:S(2)}) collective-permute-start(bf16[32,2048]{1,0:T(8,128)(2,1)S(1)} %get-tuple-element.14), channel_id=1, source_target_pairs={{8,0},{16,8},{24,16},{32,24},{40,32},{48,40},{56,48},{64,56},{72,6... | collective-permute-start | bytes 393224 | tf_op jit(solution)/shard_map/ppermute | solution.py:29
  311.0 8.8 %collective-permute-start.31 = (bf16[32,2048]{1,0:T(8,128)(2,1)S(1)}, bf16[32,2048]{1,0:T(8,128)(2,1)S(1)}, u32[]{:S(2)}, u32[]{:S(2)}) collective-permute-start(bf16[32,2048]{1,0:T(8,128)(2,1)S(1)} %get-tuple-element.15), channel_id=1, source_target_pairs={{112,0},{120,8},{0,16},{8,24},{16,32},{24,40},{32,48},{40,56},{48,... | collective-permute-start | bytes 393224 | tf_op jit(solution)/shard_map/ppermute | solution.py:29
  312.0 10.0 %collective-permute-start.30 = (bf16[32,2048]{1,0:T(8,128)(2,1)S(1)}, bf16[32,2048]{1,0:T(8,128)(2,1)S(1)}, u32[]{:S(2)}, u32[]{:S(2)}) collective-permute-start(bf16[32,2048]{1,0:T(8,128)(2,1)S(1)} %get-tuple-element.16), channel_id=1, source_target_pairs={{120,0},{0,8},{8,16},{16,24},{24,32},{32,40},{40,48},{48,56},{56,6... | collective-permute-start | bytes 393224 | tf_op jit(solution)/shard_map/ppermute | solution.py:29
  322.8 19.8 %all-to-all-start.1 = ((bf16[4,8,2048]{2,1,0:T(8,128)(2,1)}), bf16[4,8,2048]{2,1,0:T(8,128)(2,1)S(1)}, u32[]{:S(2)}, u32[]{:S(2)}) async-start(bf16[4,8,2048]{2,1,0:T(8,128)(2,1)} %fusion.20), calls=%async_computation.1 | async-start | bytes 262144 | tf_op jit(solution)/shard_map/all_to_all | solution.py:345
  (6 other events, 6.9 us)
